TPU v7x, 32 devices: a whole 2x2x4 slice. The times are simulated.
32 devices in a mesh: sp: 16 (over z, y, x), tp: 2 (over core).
Axes of the slice: x: 2, y: 2, z: 4, core: 2. Of those that a mesh axis runs over, the one named last changes fastest.
Arguments:
- tokens: bfloat16 [4096, 2048], P('sp', 'tp'), may hold values from -6 to 6
- outer_gate: bfloat16 [2048, 1024], P(None, 'tp'), may hold values from -0.125 to 0.125
- inner_gate: bfloat16 [2048, 1024], P(None, 'tp'), may hold values from -0.125 to 0.125
- conv_input: bfloat16 [2048, 1024], P(None, 'tp'), may hold values from -0.125 to 0.125
- conv_taps: bfloat16 [3, 1024], P(None, 'tp'), may hold values from -3.5 to 3.5
- query_down: bfloat16 [2048, 512], P(None, 'tp'), may hold values from -0.125 to 0.125
- latent_down: bfloat16 [2048, 256], P(None, 'tp'), may hold values from -0.125 to 0.125
- rotary_down: bfloat16 [2048, 32], replicated, may hold values from -5.303301 to 5.303301
- query_gain: float32 [512], replicated, may hold values from 0.1 to 1.9
- latent_gain: float32 [256], replicated, may hold values from 0.1 to 1.9
- query_up: bfloat16 [512, 1536], P(None, 'tp'), may hold values from -0.52734375 to 0.52734375
- latent_up: bfloat16 [256, 2048], P(None, 'tp'), may hold values from -0.75 to 0.75
- conv_project: bfloat16 [1024, 2048], P('tp'), may hold values from -0.1875 to 0.1875
- attend_project: bfloat16 [1024, 2048], P('tp'), may hold values from -0.1875 to 0.1875
Outputs:
- mixed: bfloat16 [4096, 2048], P(('sp', 'tp'))
All inputs are finite; a program needn't handle non-finite values.
Results may differ from a plain program's by a relative error of at most 0.035.
Values may be sent and summed in bfloat16 or wider, within the bound.
A program may use at most 128 MiB of HBM per device.

v0:
```python
import math

import jax
import jax.numpy as jnp
from jax import lax
from jax.sharding import PartitionSpec as P

NOPE = 64
ROPE = 32
VDIM = 64


neg_fill = -1e30
rotary_base = 10000.0
norm_epsilon = 1e-06


def shifted(shard, axis, by):
    length = lax.axis_size(axis)
    pairs = [(i, i + by) for i in range(length) if 0 <= i + by < length]
    return lax.ppermute(shard, axis, pairs)


def rotate(values, positions):
    half = values.shape[-1] // 2
    inverse = rotary_base ** (-(jnp.arange(half, dtype=jnp.float32) * 2.0 / (2 * half)))
    angle = positions[:, None] * inverse[None, :]
    if values.ndim == 3:
        angle = angle[:, None, :]
    cosine = jnp.cos(angle)
    sine = jnp.sin(angle)
    first = values[..., :half]
    second = values[..., half:]
    return jnp.concatenate([first * cosine - second * sine, first * sine + second * cosine], -1)


def rms_scale(latent, gain):
    values = latent.astype(jnp.float32)
    factor = lax.rsqrt(jnp.mean(values * values, -1, keepdims=True) + norm_epsilon)
    return (values * factor * gain).astype(jnp.bfloat16)


def local(
    tokens,
    outer_gate,
    inner_gate,
    conv_input,
    conv_taps,
    query_down,
    latent_down,
    rotary_down,
    query_gain,
    latent_gain,
    query_up,
    latent_up,
    conv_project,
    attend_project,
):
    tok_rows = tokens.shape[0]
    local_heads = query_up.shape[1] // (NOPE + ROPE)
    weights = (outer_gate, inner_gate, conv_input, query_down, latent_down, rotary_down)
    piece = lax.all_gather(tokens, "tp", axis=1, tiled=True)
    outer, inner, signal, query_part, latent_part, rotary_raw = tuple(
        (jnp.dot(piece, weight, preferred_element_type=jnp.float32) for weight in weights)
    )
    query_lat, latent_lat = (
        lax.all_gather(query_part.astype(jnp.bfloat16), "tp", axis=1, tiled=True),
        lax.all_gather(latent_part.astype(jnp.bfloat16), "tp", axis=1, tiled=True),
    )
    gated = (inner * signal).astype(jnp.bfloat16)
    reach = conv_taps.shape[0] - 1
    rim = shifted(gated[tok_rows - reach :], "sp", 1)
    padded = jnp.concatenate([rim, gated], 0).astype(jnp.float32)
    taps = conv_taps.astype(jnp.float32)
    filtered = padded[0:tok_rows] * taps[0]
    for index in range(1, reach + 1):
        filtered = filtered + padded[index : index + tok_rows] * taps[index]
    conv_result = (outer * filtered).astype(jnp.bfloat16)
    seq_index = lax.axis_index("sp")
    offset = seq_index * tok_rows
    query_index = offset + jnp.arange(tok_rows, dtype=jnp.int32)
    positions = query_index.astype(jnp.float32)
    query_norm = rms_scale(query_lat, query_gain)
    latent_norm = rms_scale(latent_lat, latent_gain)
    rotary_key = rotate(rotary_raw, positions).astype(jnp.bfloat16)
    query_full = jnp.dot(query_norm, query_up, preferred_element_type=jnp.float32)
    query_full = query_full.reshape(tok_rows, local_heads, NOPE + ROPE)
    query_plain = query_full[..., :NOPE].astype(jnp.bfloat16)
    query_rot = rotate(query_full[..., NOPE:], positions).astype(jnp.bfloat16)
    scale = (NOPE + ROPE) ** (-0.5)
    query_sets = ((query_plain, query_rot, query_index),)
    set_lasts = tuple((jnp.max(members[2]) for members in query_sets))
    overall_last = set_lasts[0]

    def update(current, members, key_plain, values, rot_block, first, block):
        plain, turned, indices = members
        best, total, accum = current
        scores = jnp.einsum("qhd,khd->hqk", plain, key_plain, preferred_element_type=jnp.float32)
        scores = scores + jnp.einsum(
            "qhr,kr->hqk", turned, rot_block, preferred_element_type=jnp.float32
        )
        scores = scores * scale
        key_index = first + jnp.arange(block, dtype=jnp.int32)
        visible = key_index[None, :] <= indices[:, None]
        scores = jnp.where(visible[None], scores, neg_fill)
        new_best = jnp.maximum(best, jnp.max(scores, -1))
        factor = jnp.exp(best - new_best)
        weight = jnp.exp(scores - new_best[..., None])
        total = total * factor + jnp.sum(weight, -1)
        accum = accum * factor[..., None] + jnp.einsum(
            "hqk,khd->hqd", weight.astype(jnp.bfloat16), values, preferred_element_type=jnp.float32
        )
        return (new_best, total, accum)

    initial = tuple(
        (
            (
                jnp.full((local_heads, members[2].shape[0]), neg_fill, jnp.float32),
                jnp.zeros((local_heads, members[2].shape[0]), jnp.float32),
                jnp.zeros((local_heads, members[2].shape[0], VDIM), jnp.float32),
            )
            for members in query_sets
        )
    )
    carry = initial
    keys_latent = lax.all_gather(latent_norm, "sp", axis=0, tiled=True)
    keys_rot = lax.all_gather(rotary_key, "sp", axis=0, tiled=True)
    count = keys_latent.shape[0]
    block = math.gcd(count, 512)
    latent_blocks = keys_latent.reshape(count // block, block, keys_latent.shape[1])
    rot_blocks = keys_rot.reshape(count // block, block, keys_rot.shape[1])

    def advance(states, inputs):
        latent_block, rot_block, number = inputs
        first = number * block

        def compute(current):
            expanded = jnp.dot(latent_block, latent_up, preferred_element_type=jnp.float32)
            expanded = expanded.astype(jnp.bfloat16).reshape(block, local_heads, NOPE + VDIM)
            key_plain = expanded[..., :NOPE]
            values = expanded[..., NOPE:]
            results = []
            for members, last, state in zip(query_sets, set_lasts, current):
                results.append(
                    lax.cond(
                        first > last,
                        lambda kept: kept,
                        lambda kept, members=members: update(
                            kept, members, key_plain, values, rot_block, first, block
                        ),
                        state,
                    )
                )
            return tuple(results)

        return (lax.cond(first > overall_last, lambda current: current, compute, states), None)

    numbers = jnp.arange(count // block, dtype=jnp.int32)
    carry, unused = lax.scan(advance, carry, (latent_blocks, rot_blocks, numbers))
    states = carry
    outputs = []
    for state in states:
        best, total, accum = state
        rows = accum.shape[1]
        outputs.append(
            (accum / total[..., None])
            .transpose(1, 0, 2)
            .reshape(rows, local_heads * VDIM)
            .astype(jnp.bfloat16)
        )
    attended = outputs[0]
    return lax.psum_scatter(
        (
            jnp.dot(conv_result, conv_project, preferred_element_type=jnp.float32)
            + jnp.dot(attended, attend_project, preferred_element_type=jnp.float32)
        ).astype(jnp.bfloat16),
        "tp",
        scatter_dimension=0,
        tiled=True,
    )


def solution(mesh):
    in_specs = (
        P("sp", "tp"),
        P(None, "tp"),
        P(None, "tp"),
        P(None, "tp"),
        P(None, "tp"),
        P(None, "tp"),
        P(None, "tp"),
        P(),
        P(),
        P(),
        P(None, "tp"),
        P(None, "tp"),
        P("tp", None),
        P("tp", None),
    )
    out_specs = P(("sp", "tp"), None)
    return jax.shard_map(local, mesh=mesh, in_specs=in_specs, out_specs=out_specs, check_vma=False)
```

profile of v0, /device:TPU:29, one launch (start us, length us, event | category | flops | bytes accessed | tf_op | source)
XLA Modules:
  0.0 228.9 jit_solution(8106722850243884223)
XLA Ops:
  7.3 12.3 %all-gather.3.cloned.1.call-done = bf16[256,2048]{1,0:T(8,128)(2,1)} async-done(((bf16[256,1024]{1,0:T(8,128)(2,1)}), bf16[256,2048]{1,0:T(8,128)(2,1)}) %all-gather.3.cloned.1.call-update) | async-done | bytes 1048592 | tf_op jit(solution)/shard_map/all_gather | solution.py:62
  19.6 1.9 convolution_convert_fusion.2
  21.5 1.9 all_gather.16
  25.1 2.4 %fusion.46 = f32[256,512]{1,0:T(8,128)S(1)} fusion(bf16[256,2048]{1,0:T(8,128)(2,1)S(1)} %copy-done.2, bf16[2048,512]{1,0:T(8,128)(2,1)} %param.22), kind=kOutput, calls=%fused_computation.75 | convolution fusion | flops 536870912 | bytes 3670016 | tf_op jit(solution)/shard_map/dot_general | solution.py:64
  28.3 3.2 %collective-permute-start = (bf16[2,512]{1,0:T(2,128)(2,1)S(1)}, bf16[2,512]{1,0:T(2,128)(2,1)S(1)}, u32[]{:S(2)}, u32[]{:S(2)}) collective-permute-start(bf16[2,512]{1,0:T(2,128)(2,1)S(1)} %slice.66), channel_id=1, source_target_pairs={{0,2},{2,4},{4,6},{6,8},{8,10},{10,12},{12,14},{14,16},{16,18},{18... | collective-permute-start | bytes 6152 | tf_op jit(solution)/shard_map/ppermute | solution.py:21
  32.0 2.1 all_gather.18
  34.7 27.5 %all_gather.19 = bf16[4096,32]{0,1:T(8,128)(2,1)S(1)} all-gather(bf16[256,32]{0,1:T(8,128)(2,1)S(1)} %pad_maximum_fusion.1), channel_id=1, replica_groups=mesh['sp'=16,'tp'=2] {'sp'}, dimensions={0}, use_global_device_ids=true | all-gather | bytes 278528 | tf_op jit(solution)/shard_map/all_gather | solution.py:127
  64.6 4.7 %fusion.24 = f32[256,2048]{1,0:T(8,128)} fusion(bf16[512,2048]{1,0:T(8,128)(2,1)S(1)} %copy-done, bf16[256,2048]{1,0:T(8,128)(2,1)S(1)} %copy-done.2, bf16[2048,512]{1,0:T(8,128)(2,1)} %param.21, f32[258,512]{1,0:T(8,128)} %maximum_convert_fusion, f32[512]{0:T(512)S(1)} %bitcast.60, f32[512]{0:T(512)S(1)} %bitcast.59, f32[512]{0:T(512)S(1)} %bitcast.58), kind=kOutput, calls=%fused_computation.32 | convolution fusion | flops 1074659328 | bytes 8919040 | tf_op jit(solution)/shard_map/dot_general | solution.py:174
  69.4 14.5 %all-gather.5.cloned.1.call-done = bf16[4096,256]{1,0:T(8,128)(2,1)} async-done(((bf16[256,256]{1,0:T(8,128)(2,1)}), bf16[4096,256]{1,0:T(8,128)(2,1)}) %all-gather.5.cloned.1.call-update) | async-done | bytes 2097168 | tf_op jit(solution)/shard_map/all_gather | solution.py:126
  85.3 121.6 %while.15 = (s32[]{:T(128)}, f32[8,256]{1,0:T(8,128)S(1)}, f32[8,256]{1,0:T(8,128)S(1)}, f32[8,256,64]{1,2,0:T(8,128)}, s32[8]{0:T(128)}, /*index=5*/s32[]{:T(12...) while((s32[]{:T(128)}, f32[8,256]{1,0:T(8,128)S(1)}, ...), condition=%wide.region_10.11_spmd.clone, body=%wide.region_3.10_spmd.clone.sunk | while | flops 613290752 | bytes 36222520 | solution.py:159
  88.3 12.1 %conditional.4 = ((f32[8,256]{1,0:T(8,128)S(1)}, f32[8,256]{1,0:T(8,128)S(1)}, f32[8,256,64]{1,2,0:T(8,128)})) conditional(s32[]{:T(128)} %convert_element_type.122, (s32[]{:T(128)}, s32[]{:T(128)}, bf16[8,512,256]{2,1,0:T(8,128)(2,1)}, s32[]{:T(128)}, bf16[256,1024]{1,0:T(8,128)(2,1)}, /*index=5*/s32[]{:T(128)}, bf16[256,8,64]{0,2,1:T(8,128)(2,1)S(1)}, ...), branch_computations={%region_4.8_spmd, %region_9.9_spmd} | conditional | flops 613290752 | bytes 36204816 | solution.py:156
  88.3 1.6 convolution_convert_fusion
  91.8 8.7 %conditional = (f32[8,256]{1,0:T(8,128)S(1)}, f32[8,256]{1,0:T(8,128)S(1)}, f32[8,256,64]{1,2,0:T(8,128)}) conditional(s32[]{:T(128)} %convert_element_type.52, (s32[]{:T(128)}, s32[256]{0:T(256)}, bf16[512,1024]{1,0:T(8,128)(2,1)S(1)}, bf16[256,8,64]{0,2,1:T(8,128)(2,1)S(1)}, bf16[8,512,32]{1,2,0:T(8,128)(2,1)}, /*index=5*/s32[]{:T(128)}, ...), branch_computations={%region_5.6_spmd, %region_8.7_spmd} | conditional | flops 344330752 | bytes 34367116 | solution.py:145
  93.2 1.8 fusion.13
  95.1 2.0 fusion.44
  103.5 12.1 %conditional.4 = ((f32[8,256]{1,0:T(8,128)S(1)}, f32[8,256]{1,0:T(8,128)S(1)}, f32[8,256,64]{1,2,0:T(8,128)})) conditional(s32[]{:T(128)} %convert_element_type.122, (s32[]{:T(128)}, s32[]{:T(128)}, bf16[8,512,256]{2,1,0:T(8,128)(2,1)}, s32[]{:T(128)}, bf16[256,1024]{1,0:T(8,128)(2,1)}, /*index=5*/s32[]{:T(128)}, bf16[256,8,64]{0,2,1:T(8,128)(2,1)S(1)}, ...), branch_computations={%region_4.8_spmd, %region_9.9_spmd} | conditional | flops 613290752 | bytes 36204816 | solution.py:156
  103.5 1.6 convolution_convert_fusion
  107.0 8.7 %conditional = (f32[8,256]{1,0:T(8,128)S(1)}, f32[8,256]{1,0:T(8,128)S(1)}, f32[8,256,64]{1,2,0:T(8,128)}) conditional(s32[]{:T(128)} %convert_element_type.52, (s32[]{:T(128)}, s32[256]{0:T(256)}, bf16[512,1024]{1,0:T(8,128)(2,1)S(1)}, bf16[256,8,64]{0,2,1:T(8,128)(2,1)S(1)}, bf16[8,512,32]{1,2,0:T(8,128)(2,1)}, /*index=5*/s32[]{:T(128)}, ...), branch_computations={%region_5.6_spmd, %region_8.7_spmd} | conditional | flops 344330752 | bytes 34367116 | solution.py:145
  108.4 1.8 fusion.13
  110.3 2.0 fusion.44
  118.7 12.1 %conditional.4 = ((f32[8,256]{1,0:T(8,128)S(1)}, f32[8,256]{1,0:T(8,128)S(1)}, f32[8,256,64]{1,2,0:T(8,128)})) conditional(s32[]{:T(128)} %convert_element_type.122, (s32[]{:T(128)}, s32[]{:T(128)}, bf16[8,512,256]{2,1,0:T(8,128)(2,1)}, s32[]{:T(128)}, bf16[256,1024]{1,0:T(8,128)(2,1)}, /*index=5*/s32[]{:T(128)}, bf16[256,8,64]{0,2,1:T(8,128)(2,1)S(1)}, ...), branch_computations={%region_4.8_spmd, %region_9.9_spmd} | conditional | flops 613290752 | bytes 36204816 | solution.py:156
  118.7 1.6 convolution_convert_fusion
  122.2 8.7 %conditional = (f32[8,256]{1,0:T(8,128)S(1)}, f32[8,256]{1,0:T(8,128)S(1)}, f32[8,256,64]{1,2,0:T(8,128)}) conditional(s32[]{:T(128)} %convert_element_type.52, (s32[]{:T(128)}, s32[256]{0:T(256)}, bf16[512,1024]{1,0:T(8,128)(2,1)S(1)}, bf16[256,8,64]{0,2,1:T(8,128)(2,1)S(1)}, bf16[8,512,32]{1,2,0:T(8,128)(2,1)}, /*index=5*/s32[]{:T(128)}, ...), branch_computations={%region_5.6_spmd, %region_8.7_spmd} | conditional | flops 344330752 | bytes 34367116 | solution.py:145
  123.6 1.8 fusion.13
  125.5 2.0 fusion.44
  133.9 12.1 %conditional.4 = ((f32[8,256]{1,0:T(8,128)S(1)}, f32[8,256]{1,0:T(8,128)S(1)}, f32[8,256,64]{1,2,0:T(8,128)})) conditional(s32[]{:T(128)} %convert_element_type.122, (s32[]{:T(128)}, s32[]{:T(128)}, bf16[8,512,256]{2,1,0:T(8,128)(2,1)}, s32[]{:T(128)}, bf16[256,1024]{1,0:T(8,128)(2,1)}, /*index=5*/s32[]{:T(128)}, bf16[256,8,64]{0,2,1:T(8,128)(2,1)S(1)}, ...), branch_computations={%region_4.8_spmd, %region_9.9_spmd} | conditional | flops 613290752 | bytes 36204816 | solution.py:156
  133.9 1.6 convolution_convert_fusion
  137.4 8.7 %conditional = (f32[8,256]{1,0:T(8,128)S(1)}, f32[8,256]{1,0:T(8,128)S(1)}, f32[8,256,64]{1,2,0:T(8,128)}) conditional(s32[]{:T(128)} %convert_element_type.52, (s32[]{:T(128)}, s32[256]{0:T(256)}, bf16[512,1024]{1,0:T(8,128)(2,1)S(1)}, bf16[256,8,64]{0,2,1:T(8,128)(2,1)S(1)}, bf16[8,512,32]{1,2,0:T(8,128)(2,1)}, /*index=5*/s32[]{:T(128)}, ...), branch_computations={%region_5.6_spmd, %region_8.7_spmd} | conditional | flops 344330752 | bytes 34367116 | solution.py:145
  138.8 1.8 fusion.13
  140.7 2.0 fusion.44
  149.1 12.1 %conditional.4 = ((f32[8,256]{1,0:T(8,128)S(1)}, f32[8,256]{1,0:T(8,128)S(1)}, f32[8,256,64]{1,2,0:T(8,128)})) conditional(s32[]{:T(128)} %convert_element_type.122, (s32[]{:T(128)}, s32[]{:T(128)}, bf16[8,512,256]{2,1,0:T(8,128)(2,1)}, s32[]{:T(128)}, bf16[256,1024]{1,0:T(8,128)(2,1)}, /*index=5*/s32[]{:T(128)}, bf16[256,8,64]{0,2,1:T(8,128)(2,1)S(1)}, ...), branch_computations={%region_4.8_spmd, %region_9.9_spmd} | conditional | flops 613290752 | bytes 36204816 | solution.py:156
  152.6 8.7 %conditional = (f32[8,256]{1,0:T(8,128)S(1)}, f32[8,256]{1,0:T(8,128)S(1)}, f32[8,256,64]{1,2,0:T(8,128)}) conditional(s32[]{:T(128)} %convert_element_type.52, (s32[]{:T(128)}, s32[256]{0:T(256)}, bf16[512,1024]{1,0:T(8,128)(2,1)S(1)}, bf16[256,8,64]{0,2,1:T(8,128)(2,1)S(1)}, bf16[8,512,32]{1,2,0:T(8,128)(2,1)}, /*index=5*/s32[]{:T(128)}, ...), branch_computations={%region_5.6_spmd, %region_8.7_spmd} | conditional | flops 344330752 | bytes 34367116 | solution.py:145
  154.0 1.8 fusion.13
  155.9 2.0 fusion.44
  164.3 12.1 %conditional.4 = ((f32[8,256]{1,0:T(8,128)S(1)}, f32[8,256]{1,0:T(8,128)S(1)}, f32[8,256,64]{1,2,0:T(8,128)})) conditional(s32[]{:T(128)} %convert_element_type.122, (s32[]{:T(128)}, s32[]{:T(128)}, bf16[8,512,256]{2,1,0:T(8,128)(2,1)}, s32[]{:T(128)}, bf16[256,1024]{1,0:T(8,128)(2,1)}, /*index=5*/s32[]{:T(128)}, bf16[256,8,64]{0,2,1:T(8,128)(2,1)S(1)}, ...), branch_computations={%region_4.8_spmd, %region_9.9_spmd} | conditional | flops 613290752 | bytes 36204816 | solution.py:156
  167.8 8.7 %conditional = (f32[8,256]{1,0:T(8,128)S(1)}, f32[8,256]{1,0:T(8,128)S(1)}, f32[8,256,64]{1,2,0:T(8,128)}) conditional(s32[]{:T(128)} %convert_element_type.52, (s32[]{:T(128)}, s32[256]{0:T(256)}, bf16[512,1024]{1,0:T(8,128)(2,1)S(1)}, bf16[256,8,64]{0,2,1:T(8,128)(2,1)S(1)}, bf16[8,512,32]{1,2,0:T(8,128)(2,1)}, /*index=5*/s32[]{:T(128)}, ...), branch_computations={%region_5.6_spmd, %region_8.7_spmd} | conditional | flops 344330752 | bytes 34367116 | solution.py:145
  169.2 1.8 fusion.13
  171.1 2.0 fusion.44
  179.5 12.1 %conditional.4 = ((f32[8,256]{1,0:T(8,128)S(1)}, f32[8,256]{1,0:T(8,128)S(1)}, f32[8,256,64]{1,2,0:T(8,128)})) conditional(s32[]{:T(128)} %convert_element_type.122, (s32[]{:T(128)}, s32[]{:T(128)}, bf16[8,512,256]{2,1,0:T(8,128)(2,1)}, s32[]{:T(128)}, bf16[256,1024]{1,0:T(8,128)(2,1)}, /*index=5*/s32[]{:T(128)}, bf16[256,8,64]{0,2,1:T(8,128)(2,1)S(1)}, ...), branch_computations={%region_4.8_spmd, %region_9.9_spmd} | conditional | flops 613290752 | bytes 36204816 | solution.py:156
  183.0 8.7 %conditional = (f32[8,256]{1,0:T(8,128)S(1)}, f32[8,256]{1,0:T(8,128)S(1)}, f32[8,256,64]{1,2,0:T(8,128)}) conditional(s32[]{:T(128)} %convert_element_type.52, (s32[]{:T(128)}, s32[256]{0:T(256)}, bf16[512,1024]{1,0:T(8,128)(2,1)S(1)}, bf16[256,8,64]{0,2,1:T(8,128)(2,1)S(1)}, bf16[8,512,32]{1,2,0:T(8,128)(2,1)}, /*index=5*/s32[]{:T(128)}, ...), branch_computations={%region_5.6_spmd, %region_8.7_spmd} | conditional | flops 344330752 | bytes 34367116 | solution.py:145
  184.4 1.8 fusion.13
  186.3 2.0 fusion.44
  194.7 12.1 %conditional.4 = ((f32[8,256]{1,0:T(8,128)S(1)}, f32[8,256]{1,0:T(8,128)S(1)}, f32[8,256,64]{1,2,0:T(8,128)})) conditional(s32[]{:T(128)} %convert_element_type.122, (s32[]{:T(128)}, s32[]{:T(128)}, bf16[8,512,256]{2,1,0:T(8,128)(2,1)}, s32[]{:T(128)}, bf16[256,1024]{1,0:T(8,128)(2,1)}, /*index=5*/s32[]{:T(128)}, bf16[256,8,64]{0,2,1:T(8,128)(2,1)S(1)}, ...), branch_computations={%region_4.8_spmd, %region_9.9_spmd} | conditional | flops 613290752 | bytes 36204816 | solution.py:156
  198.2 8.7 %conditional = (f32[8,256]{1,0:T(8,128)S(1)}, f32[8,256]{1,0:T(8,128)S(1)}, f32[8,256,64]{1,2,0:T(8,128)}) conditional(s32[]{:T(128)} %convert_element_type.52, (s32[]{:T(128)}, s32[256]{0:T(256)}, bf16[512,1024]{1,0:T(8,128)(2,1)S(1)}, bf16[256,8,64]{0,2,1:T(8,128)(2,1)S(1)}, bf16[8,512,32]{1,2,0:T(8,128)(2,1)}, /*index=5*/s32[]{:T(128)}, ...), branch_computations={%region_5.6_spmd, %region_8.7_spmd} | conditional | flops 344330752 | bytes 34367116 | solution.py:145
  199.6 1.8 fusion.13
  201.5 2.0 fusion.44
  207.9 3.9 %fusion.21 = bf16[256,2048]{1,0:T(8,128)(2,1)} fusion(f32[256,2048]{1,0:T(8,128)} %fusion.24, bf16[256,512]{0,1:T(8,128)(2,1)S(1)} %bitcast.55, bf16[512,2048]{1,0:T(8,128)(2,1)} %param.33), kind=kOutput, calls=%fused_computation.26 | convolution fusion | flops 537919488 | bytes 5505024 | tf_op jit(solution)/shard_map/dot_general | solution.py:175
  211.9 10.5 %reduce-scatter.2.cloned.1.call-done = bf16[128,2048]{1,0:T(8,128)(2,1)} async-done(((bf16[256,2048]{1,0:T(8,128)(2,1)}), bf16[128,2048]{1,0:T(8,128)(2,1)}) %reduce-scatter.2.cloned.1.call-update) | async-done | bytes 524304 | tf_op jit(solution)/shard_map/reduce_scatter | solution.py:172
  (207 shorter events, 78.4 us)
Async XLA Ops:
  6.5 58.1 %copy-start = (bf16[512,2048]{1,0:T(8,128)(2,1)S(1)}, bf16[512,2048]{1,0:T(8,128)(2,1)}, u32[]{:S(2)}) copy-start(bf16[512,2048]{1,0:T(8,128)(2,1)} %param.32) | copy-start | bytes 6291460
  6.5 17.0 %copy-start.12 = (f32[256]{0:T(256)S(1)}, f32[256]{0:T(256)}, u32[]{:S(2)}) copy-start(f32[256]{0:T(256)} %param.29) | copy-start | bytes 3076
  6.5 18.5 %copy-start.10 = (bf16[3,512]{1,0:T(4,128)(2,1)S(1)}, bf16[3,512]{1,0:T(4,128)(2,1)}, u32[]{:S(2)}) copy-start(bf16[3,512]{1,0:T(4,128)(2,1)} %param.24) | copy-start | bytes 9220
  6.5 13.1 %all-gather.3.cloned.1.call-start = ((), (), s32[]{:S(2)}) async-start(), calls=%async_computation.1 | async-start | bytes 1572864 | tf_op jit(solution)/shard_map/all_gather | solution.py:62
  7.3 76.6 %all-gather.5.cloned.1.call-start = ((), (), s32[]{:S(2)}) async-start(), calls=%async_computation.2 | async-start | bytes 2228224 | tf_op jit(solution)/shard_map/all_gather | solution.py:126
  19.6 5.5 %copy-start.2 = (bf16[256,2048]{1,0:T(8,128)(2,1)S(1)}, bf16[256,2048]{1,0:T(8,128)(2,1)}, u32[]{:S(2)}) copy-start(bf16[256,2048]{1,0:T(8,128)(2,1)} %all-gather.3.cloned.1.call-done) | copy-start | bytes 3145732
  24.3 198.0 %reduce-scatter.2.cloned.1.call-start = ((), (), s32[]{:S(2)}) async-start(), calls=%async_computation.3 | async-start | bytes 1572864 | tf_op jit(solution)/shard_map/reduce_scatter | solution.py:172
  25.0 2.5 %copy-start.5 = (bf16[2048,512]{1,0:T(8,128)(2,1)S(1)}, bf16[2048,512]{1,0:T(8,128)(2,1)}, u32[]{:S(2)}) copy-start(bf16[2048,512]{1,0:T(8,128)(2,1)} %param.23) | copy-start | bytes 6291460
  27.5 4.0 %copy-start.6 = (bf16[2048,256]{1,0:T(8,128)(2,1)S(1)}, bf16[2048,256]{1,0:T(8,128)(2,1)}, u32[]{:S(2)}) copy-start(bf16[2048,256]{1,0:T(8,128)(2,1)} %param.25) | copy-start | bytes 3145732
  28.3 5.9 %copy-start.8 = (bf16[2048,32]{0,1:T(8,128)(2,1)S(1)}, bf16[2048,32]{0,1:T(8,128)(2,1)}, u32[]{:S(2)}) copy-start(bf16[2048,32]{0,1:T(8,128)(2,1)} %param.27) | copy-start | bytes 393220
  28.3 34.1 %copy-start.7 = (bf16[512,768]{1,0:T(8,128)(2,1)S(1)}, bf16[512,768]{1,0:T(8,128)(2,1)}, u32[]{:S(2)}) copy-start(bf16[512,768]{1,0:T(8,128)(2,1)} %param.30) | copy-start | bytes 2359300
  28.3 34.1 %copy-start.11 = (f32[512]{0:T(512)S(1)}, f32[512]{0:T(512)}, u32[]{:S(2)}) copy-start(f32[512]{0:T(512)} %param.28) | copy-start | bytes 6148
  28.3 35.4 %collective-permute-start = (bf16[2,512]{1,0:T(2,128)(2,1)S(1)}, bf16[2,512]{1,0:T(2,128)(2,1)S(1)}, u32[]{:S(2)}, u32[]{:S(2)}) collective-permute-start(bf16[2,512]{1,0:T(2,128)(2,1)S(1)} %slice.66), channel_id=1, source_target_pairs={{0,2},{2,4},{4,6},{6,8},{8,10},{10,12},{12,14},{14,16},{16,18},{18... | collective-permute-start | bytes 6152 | tf_op jit(solution)/shard_map/ppermute | solution.py:21
  93.2 1.8 copy-start.9
  97.1 1.2 copy-start.1
  97.1 1.3 copy-start.3
  99.7 0.8 copy-start.4
  108.4 1.8 copy-start.9
  112.3 1.2 copy-start.1
  112.3 1.3 copy-start.3
  114.9 0.8 copy-start.4
  123.6 1.8 copy-start.9
  127.5 1.2 copy-start.1
  127.5 1.3 copy-start.3
  130.1 0.8 copy-start.4
  138.8 1.8 copy-start.9
  142.7 1.2 copy-start.1
  142.7 1.3 copy-start.3
  145.3 0.8 copy-start.4
  154.0 1.8 copy-start.9
  157.9 1.2 copy-start.1
  157.9 1.3 copy-start.3
  160.5 0.8 copy-start.4
  169.2 1.8 copy-start.9
  173.1 1.2 copy-start.1
  173.1 1.3 copy-start.3
  175.7 0.8 copy-start.4
  184.4 1.8 copy-start.9
  188.3 1.2 copy-start.1
  188.3 1.3 copy-start.3
  190.9 0.8 copy-start.4
  199.6 1.8 copy-start.9
  203.5 1.2 copy-start.1
  203.5 1.3 copy-start.3
  206.1 0.8 copy-start.4
Sparse Core Ops, SparseCore 0:
  8.9 10.6 all-gather.2
  24.4 59.3 all-gather.4
  212.0 10.2 reduce-scatter.1
where the time goes:
time: 232 us; the launch traced here: 229 us
  matrix products  67.2 us (29%)
  waiting for transfers between devices  38 us (16%)
  local copies, waits for them, and re-layouts  36 us (16%)
  blocking collectives  31.5 us (14%)
  other arithmetic  23.7 us (10%)
  loops' own time  15.8 us (7%)
  between operations  13.3 us (6%)
  starting transfers between devices  3.31 us (1%)
    all_gather x1, blocking collectives, local(): keys_rot = lax.all_gather(rotary_key, 'sp', axis=0, tiled=True)  27.5 us
    dot_general x8, matrix products, update(): jnp.einsum('qhr,kr->hqk', turned, rot_block, preferred_element_type=jnp.f...  15.8 us
    all_gather x1, waiting for transfers between devices, local(): keys_latent = lax.all_gather(latent_norm, 'sp', axis=0, tiled=True)  14.5 us
    dot_general x8, matrix products, update(): jnp.einsum('qhd,khd->hqk', plain, key_plain, preferred_element_type=jnp.f...  14.4 us
    dot_general x8, matrix products, compute(): jnp.dot(latent_block, latent_up, preferred_element_type=jnp.float32)  12.5 us
    all_gather x1, waiting for transfers between devices, local(): piece = lax.all_gather(tokens, 'tp', axis=1, tiled=True)  12.3 us
    another operation x8, local copies, waits for them, and re-layouts  10.7 us
    reduce_scatter x1, waiting for transfers between devices, local(): lax.psum_scatter((jnp.dot(conv_result, conv_project, preferred_element_ty...  10.5 us
  transfers between devices with their start and end apart: 4, of which 3 were waited for; matrix products, arithmetic and copies ran while one was open for 5% of the time, Pallas kernels for 0%

commit v1 on v0

v1 whole, which is shorter than its diff:
```python
import jax
import jax.numpy as jnp
from jax import lax
from jax.experimental import pallas as pl
from jax.experimental.pallas import tpu as pltpu
from jax.sharding import PartitionSpec as P

NOPE = 64
ROPE = 32
VDIM = 64
LANES = 128
ONES = 16

neg_fill = -1e30
rotary_base = 10000.0
norm_epsilon = 1e-06
log2e = 1.4426950408889634


def shifted(shard, axis, by):
    length = lax.axis_size(axis)
    pairs = [(i, i + by) for i in range(length) if 0 <= i + by < length]
    return lax.ppermute(shard, axis, pairs)


def angles(positions):
    half = ROPE // 2
    inverse = rotary_base ** (-(jnp.arange(half, dtype=jnp.float32) * 2.0 / (2 * half)))
    return positions[:, None] * inverse[None, :]


def rotate(values, positions):
    half = values.shape[-1] // 2
    angle = angles(positions)
    if values.ndim == 3:
        angle = angle[:, None, :]
    cosine = jnp.cos(angle)
    sine = jnp.sin(angle)
    first = values[..., :half]
    second = values[..., half:]
    return jnp.concatenate([first * cosine - second * sine, first * sine + second * cosine], -1)


def rms_scale(latent, gain):
    values = latent.astype(jnp.float32)
    factor = lax.rsqrt(jnp.mean(values * values, -1, keepdims=True) + norm_epsilon)
    return (values * factor * gain).astype(jnp.bfloat16)


def dot(a, b, dims=((1,), (0,))):
    return lax.dot_general(a, b, (dims, ((), ())), preferred_element_type=jnp.float32)


def attend(lat, rot, qx_ref, up_ref, wvt_ref, best_ref, acc_ref, masked):
    heads = qx_ref.shape[0]
    expanded = dot(lat, up_ref[...]).astype(jnp.bfloat16)
    turned = dot(wvt_ref[...], lat, ((1,), (1,))).astype(jnp.bfloat16)
    ones = jnp.ones((ONES, lat.shape[0]), jnp.bfloat16)
    width = NOPE + VDIM
    for h in range(heads):
        key = jnp.concatenate([expanded[:, h * width : (h + 1) * width], rot], 1)
        s = dot(key, qx_ref[h])
        if masked:
            k_at = lax.broadcasted_iota(jnp.int32, s.shape, 0)
            q_at = lax.broadcasted_iota(jnp.int32, s.shape, 1)
            s = jnp.where(k_at <= q_at, s, neg_fill)
        values = jnp.concatenate([turned[h * VDIM : (h + 1) * VDIM], ones], 0)
        top = jnp.max(s, 0, keepdims=True)
        if masked:
            weight = jnp.exp2(s - top).astype(jnp.bfloat16)
            acc_ref[h] = dot(values, weight)
            best_ref[h] = top
        else:
            old = best_ref[h]
            new = jnp.maximum(old, top)
            weight = jnp.exp2(s - new).astype(jnp.bfloat16)
            acc_ref[h] = acc_ref[h] * jnp.exp2(old - new) + dot(values, weight)
            best_ref[h] = new


def attention_kernel(lat_ref, rot_ref, qx_ref, up_ref, wvt_ref, out_ref, best_ref, acc_ref):
    me = lax.axis_index("sp")
    rows = qx_ref.shape[2]

    def block(j, masked):
        at = pl.ds(pl.multiple_of(j * rows, rows), rows)
        attend(lat_ref[at, :], rot_ref[at, :], qx_ref, up_ref, wvt_ref, best_ref, acc_ref, masked)

    block(me, True)

    @pl.loop(0, me)
    def _(j):
        block(j, False)

    for h in range(qx_ref.shape[0]):
        acc = acc_ref[h]
        out_ref[h * VDIM : (h + 1) * VDIM, :] = (acc[:VDIM] / acc[VDIM : VDIM + 1]).astype(jnp.bfloat16)


def local(
    tokens,
    outer_gate,
    inner_gate,
    conv_input,
    conv_taps,
    query_down,
    latent_down,
    rotary_down,
    query_gain,
    latent_gain,
    query_up,
    latent_up,
    conv_project,
    attend_project,
):
    rows = tokens.shape[0]
    heads = query_up.shape[1] // (NOPE + ROPE)
    weights = (outer_gate, inner_gate, conv_input, query_down, latent_down, rotary_down)
    piece = lax.all_gather(tokens, "tp", axis=1, tiled=True)
    outer, inner, signal, query_part, latent_part, rotary_raw = tuple(
        (jnp.dot(piece, weight, preferred_element_type=jnp.float32) for weight in weights)
    )
    query_lat = lax.all_gather(query_part.astype(jnp.bfloat16), "tp", axis=1, tiled=True)
    latent_lat = lax.all_gather(latent_part.astype(jnp.bfloat16), "tp", axis=1, tiled=True)
    gated = (inner * signal).astype(jnp.bfloat16)
    reach = conv_taps.shape[0] - 1
    rim = shifted(gated[rows - reach :], "sp", 1)
    padded = jnp.concatenate([rim, gated], 0).astype(jnp.float32)
    taps = conv_taps.astype(jnp.float32)
    filtered = padded[0:rows] * taps[0]
    for index in range(1, reach + 1):
        filtered = filtered + padded[index : index + rows] * taps[index]
    conv_result = (outer * filtered).astype(jnp.bfloat16)
    positions = (lax.axis_index("sp") * rows + jnp.arange(rows, dtype=jnp.int32)).astype(jnp.float32)
    query_norm = rms_scale(query_lat, query_gain)
    latent_norm = rms_scale(latent_lat, latent_gain)
    rotary_key = rotate(rotary_raw, positions).astype(jnp.bfloat16)
    scale = (NOPE + ROPE) ** (-0.5) * log2e
    query = jnp.dot(query_norm, query_up, preferred_element_type=jnp.float32) * scale
    query = query.reshape(rows, heads, NOPE + ROPE)
    plain = query[..., :NOPE].astype(jnp.bfloat16)
    turned = rotate(query[..., NOPE:], positions).astype(jnp.bfloat16)
    qx = jnp.concatenate(
        [
            plain,
            jnp.zeros((rows, heads, VDIM), jnp.bfloat16),
            turned,
            jnp.zeros((rows, heads, LANES - ROPE), jnp.bfloat16),
        ],
        2,
    ).transpose(1, 2, 0)
    shared = jnp.concatenate([latent_norm, rotary_key], 1)
    shared = lax.all_gather(shared, "sp", axis=0, tiled=True)
    kvr = latent_norm.shape[1]
    keys = shared[:, :kvr]
    rots = jnp.pad(shared[:, kvr:], ((0, 0), (0, LANES - ROPE)))
    wvt = latent_up.reshape(kvr, heads, NOPE + VDIM)[..., NOPE:].reshape(kvr, heads * VDIM).T
    vmem = pl.BlockSpec(memory_space=pltpu.VMEM)
    attended = pl.pallas_call(
        attention_kernel,
        out_shape=jax.ShapeDtypeStruct((heads * VDIM, rows), jnp.bfloat16),
        in_specs=[vmem] * 5,
        out_specs=vmem,
        scratch_shapes=[
            pltpu.VMEM((heads, 1, rows), jnp.float32),
            pltpu.VMEM((heads, VDIM + ONES, rows), jnp.float32),
        ],
        compiler_params=pltpu.CompilerParams(vmem_limit_bytes=48 * 1024 * 1024),
    )(keys, rots, qx, latent_up, wvt)
    partial = jnp.dot(conv_result, conv_project, preferred_element_type=jnp.float32)
    partial = partial + dot(attended, attend_project, ((0,), (0,)))
    return lax.psum_scatter(partial.astype(jnp.bfloat16), "tp", scatter_dimension=0, tiled=True)


def solution(mesh):
    split = P(None, "tp")
    in_specs = (P("sp", "tp"),) + (split,) * 6 + (P(),) * 3 + (split,) * 2 + (P("tp", None),) * 2
    out_specs = P(("sp", "tp"), None)
    return jax.shard_map(local, mesh=mesh, in_specs=in_specs, out_specs=out_specs, check_vma=False)
```

time: 232 us -> 156 us (0.67)
  matrix products: 67.2 us -> 16.3 us
  Pallas kernels: 0 us -> 37.6 us
  waiting for transfers between devices: 38 us -> 70 us
  local copies, waits for them, and re-layouts: 36 us -> 7.3 us
  blocking collectives: 31.5 us -> 4.06 us
  other arithmetic: 23.7 us -> 2.49 us
  loops' own time: 15.8 us -> 0 us
    dot_general x34 -> x2, matrix products: 56.6 us -> 3.72 us  [the longest x1 1.99 us: local(): jnp.dot(query_norm, query_up, preferred_element_type=jnp.float32) * scale]
    pallas_call x0 -> x1, Pallas kernels: none -> 37.6 us  [local(): pl.pallas_call(attention_kernel, out_shape=jax.ShapeDtypeStruct((heads *...]
    all_gather x1, waiting for transfers between devices: 14.5 us -> 43.7 us  [local(): shared = lax.all_gather(shared, 'sp', axis=0, tiled=True)]
    all_gather x1 -> x0, blocking collectives: 27.5 us -> none  [local(): keys_rot = lax.all_gather(rotary_key, 'sp', axis=0, tiled=True)]
    another operation x17 -> x0, loops' own time: 15.8 us -> none  [the longest x1 9.81 us: local(): lax.scan(advance, carry, (latent_blocks, rot_blocks, numbers))]
    another operation x8 -> x0, local copies, waits for them, and re-layouts: 10.7 us -> none
    dynamic_slice x8 -> x0, local copies, waits for them, and re-layouts: 10.1 us -> none  [local(): lax.scan(advance, carry, (latent_blocks, rot_blocks, numbers))]
    add x24 -> x0, other arithmetic: 10.1 us -> none  [the longest x8 10 us: local(): query_index = offset + jnp.arange(tok_rows, dtype=jnp.int32)]
  transfers between devices with their start and end apart: 4 -> 4, of which waited for: 3 -> 4; matrix products, arithmetic and copies ran while one was open for 5% -> 10% of each run, Pallas kernels for 0% -> 0%
where the time goes in v1:
time: 156 us; the launch traced here: 154 us
  waiting for transfers between devices  70 us (45%)
  Pallas kernels  37.6 us (24%)
  matrix products  16.3 us (10%)
  between operations  13.4 us (9%)
  local copies, waits for them, and re-layouts  7.3 us (5%)
  blocking collectives  4.06 us (3%)
  starting transfers between devices  3.17 us (2%)
  other arithmetic  2.49 us (2%)
    all_gather x1, waiting for transfers between devices, local(): shared = lax.all_gather(shared, 'sp', axis=0, tiled=True)  43.7 us
    pallas_call x1, Pallas kernels, local(): pl.pallas_call(attention_kernel, out_shape=jax.ShapeDtypeStruct((heads *...  37.6 us
    reduce_scatter x1, waiting for transfers between devices, local(): lax.psum_scatter(partial.astype(jnp.bfloat16), 'tp', scatter_dimension=0,...  12.3 us
    all_gather x1, waiting for transfers between devices, local(): piece = lax.all_gather(tokens, 'tp', axis=1, tiled=True)  12.2 us
    dot_general x5, matrix products, local(): jnp.dot(piece, weight, preferred_element_type=jnp.float32)  7.87 us
    dot_general x1, matrix products, local(): jnp.dot(conv_result, conv_project, preferred_element_type=jnp.float32)  4.67 us
  transfers between devices with their start and end apart: 4, of which 4 were waited for; matrix products, arithmetic and copies ran while one was open for 10% of the time, Pallas kernels for 0%

profile of v1, /device:TPU:29, one launch (start us, length us, event | category | flops | bytes accessed | tf_op | source)
XLA Modules:
  0.0 154.3 jit_solution(17323635326472481698)
XLA Ops:
  6.5 0.0 copy-start
  6.5 0.0 all-gather.3.cloned.1.call-start
  6.5 0.7 all-gather.3.cloned.1.call-update
  7.3 0.0 all-gather.5.cloned.1.call-start
  7.3 0.0 copy-start.1
  7.4 12.2 %all-gather.3.cloned.1.call-done = bf16[256,2048]{1,0:T(8,128)(2,1)} async-done(((bf16[256,1024]{1,0:T(8,128)(2,1)}), bf16[256,2048]{1,0:T(8,128)(2,1)}) %all-gather.3.cloned.1.call-update) | async-done | bytes 1048592 | tf_op jit(solution)/shard_map/all_gather | solution.py:119
  19.6 1.9 %convolution_convert_fusion.1 = bf16[256,128]{1,0:T(8,128)(2,1)S(1)} fusion(bf16[256,2048]{1,0:T(8,128)(2,1)} %all-gather.3.cloned.1.call-done, bf16[2048,128]{1,0:T(8,128)(2,1)} %param.20), kind=kOutput, calls=%fused_computation.9 | convolution fusion | flops 134250496 | bytes 1638400 | tf_op jit(solution)/shard_map/dot_general | solution.py:121
  21.5 1.9 %all_gather.13 = bf16[256,256]{1,0:T(8,128)(2,1)S(1)} all-gather(bf16[256,128]{1,0:T(8,128)(2,1)S(1)} %convolution_convert_fusion.1), channel_id=1, replica_groups=mesh['sp'=16,'tp'=2] {'tp'}, dimensions={1}, use_global_device_ids=true | all-gather | bytes 196608 | tf_op jit(solution)/shard_map/all_gather | solution.py:124
  23.4 0.1 fusion.11
  23.5 0.0 copy-done.15
  23.5 0.1 fusion.13
  23.6 0.0 copy-done.13
  23.7 0.0 copy-done.4
  23.7 0.0 copy-start.14
  23.7 0.4 fusion.25
  24.1 1.2 multiply_cosine_fusion
  25.3 0.8 pad_maximum_fusion
  26.1 0.0 all-gather.5.cloned.1.call-update
  26.1 0.0 reduce-scatter.2.cloned.1.call-start
  26.2 0.0 copy-done.1
  26.2 0.2 copy.29
  26.4 0.0 copy-start.11
  26.4 0.0 copy-done.14
  26.5 2.0 %convolution_convert_fusion = bf16[256,256]{1,0:T(8,128)(2,1)S(1)} fusion(bf16[256,2048]{1,0:T(8,128)(2,1)} %all-gather.3.cloned.1.call-done, bf16[2048,256]{1,0:T(8,128)(2,1)} %param.19), kind=kOutput, calls=%fused_computation.7 | convolution fusion | flops 268500992 | bytes 2228224 | tf_op jit(solution)/shard_map/dot_general | solution.py:121
  28.5 2.1 %all_gather.15 = bf16[256,512]{1,0:T(8,128)(2,1)S(1)} all-gather(bf16[256,256]{1,0:T(8,128)(2,1)S(1)} %convolution_convert_fusion), channel_id=1, replica_groups=mesh['sp'=16,'tp'=2] {'tp'}, dimensions={1}, use_global_device_ids=true | all-gather | bytes 393216 | tf_op jit(solution)/shard_map/all_gather | solution.py:123
  30.6 0.1 fusion.4
  30.8 2.0 %convolution_multiply_fusion = f32[256,768]{1,0:T(8,128)} fusion(bf16[512,768]{1,0:T(8,128)(2,1)S(1)} %copy-done.11, bf16[256,512]{1,0:T(8,128)(2,1)S(1)} %all_gather.15, f32[512]{0:T(512)} %param.22, f32[256]{0:T(256)S(1)} %add_rsqrt_fusion), kind=kOutput, calls=%fused_computation.2 | convolution fusion | flops 202047488 | bytes 1838080 | tf_op jit(solution)/shard_map/dot_general | solution.py:139
  32.8 2.3 %copy.24 = f32[256,768]{0,1:T(8,128)} copy(f32[256,768]{1,0:T(8,128)} %convolution_multiply_fusion) | data formatting | bytes 1572864 | tf_op jit(solution)/shard_map/mul | solution.py:139
  35.1 0.1 copy.25
  35.1 0.1 copy.26
  35.2 2.8 %fusion.24 = f32[256,512]{1,0:T(8,128)S(1)} fusion(bf16[256,2048]{1,0:T(8,128)(2,1)} %all-gather.3.cloned.1.call-done, bf16[2048,512]{1,0:T(8,128)(2,1)} %param.16), kind=kOutput, calls=%fused_computation.49 | convolution fusion | flops 536870912 | bytes 3670016 | tf_op jit(solution)/shard_map/dot_general | solution.py:121
  38.1 0.1 copy-done.10
  38.2 0.7 fusion.2
  38.9 3.1 %collective-permute-start = (bf16[2,512]{1,0:T(2,128)(2,1)S(1)}, bf16[2,512]{1,0:T(2,128)(2,1)S(1)}, u32[]{:S(2)}, u32[]{:S(2)}) collective-permute-start(bf16[2,512]{1,0:T(2,128)(2,1)S(1)} %slice.64), channel_id=1, source_target_pairs={{0,2},{2,4},{4,6},{6,8},{8,10},{10,12},{12,14},{14,16},{16,18},{18... | collective-permute-start | bytes 6152 | tf_op jit(solution)/shard_map/ppermute | solution.py:23
  42.2 1.0 copy-done.2
  43.2 1.0 collective-permute-done
  44.1 0.1 maximum_convert_fusion
  44.2 4.7 %fusion.3 = f32[256,2048]{1,0:T(8,128)} fusion(bf16[512,2048]{1,0:T(8,128)(2,1)S(1)} %copy-done, bf16[256,2048]{1,0:T(8,128)(2,1)} %all-gather.3.cloned.1.call-done, bf16[2048,512]{1,0:T(8,128)(2,1)} %param.15, f32[258,512]{1,0:T(8,128)S(1)} %maximum_convert_fusion, f32[512]{0:T(512)S(1)} %bitcast.33, f32[512]{0:T(512)S(1)} %bitcast.32, f32[512]{0:T(512)S(1)} %bitcast.31), kind=kOutput, calls=%fused_computation.8 | convolution fusion | flops 1074659328 | bytes 8919040 | tf_op jit(solution)/shard_map/dot_general | solution.py:170
  48.9 43.7 %all-gather.5.cloned.1.call-done = bf16[4096,288]{1,0:T(8,128)(2,1)} async-done(((bf16[256,288]{1,0:T(8,128)(2,1)}), bf16[4096,288]{1,0:T(8,128)(2,1)}) %all-gather.5.cloned.1.call-update) | async-done | bytes 2359312 | tf_op jit(solution)/shard_map/all_gather | solution.py:153
  92.6 1.2 slice-done
  93.8 0.2 pad.4.rot_ref
  94.0 0.8 copy-done.7
  94.8 0.1 slice.73.lat_ref
  94.9 1.1 copy-done.3
  96.0 37.6 %shard_map.136 = bf16[512,256]{1,0:T(8,128)(2,1)S(1)} custom-call(bf16[4096,256]{1,0:T(8,128)(2,1)S(1)} %slice.73.lat_ref, bf16[4096,128]{1,0:T(8,128)(2,1)S(1)} %pad.4.rot_ref, bf16[8,256,256]{2,1,0:T(8,128)(2,1)S(1)} %bitcast.25, bf16[256,1024]{1,0:T(8,128)(2,1)S(1)} %copy-done.1, bf16[512,256]{1,0:T(8,128)(2,1)S(1)} %bitcast.26), custom_call_target="tpu_custom_call" | custom-call | tf_op jit(solution)/shard_map/pallas_call | solution.py:159
  133.7 1.7 %fusion = bf16[256,2048]{1,0:T(8,128)(2,1)} fusion(f32[256,2048]{1,0:T(8,128)S(1)} %copy-done.6, bf16[512,256]{1,0:T(8,128)(2,1)S(1)} %shard_map.136, bf16[512,2048]{1,0:T(8,128)(2,1)S(1)} %copy-done.9), kind=kOutput, calls=%fused_computation.1 | convolution fusion | flops 537919488 | bytes 5505024 | tf_op jit(solution)/shard_map/dot_general | solution.py:51
  135.4 0.0 reduce-scatter.2.cloned.1.call-update
  135.4 12.3 %reduce-scatter.2.cloned.1.call-done = bf16[128,2048]{1,0:T(8,128)(2,1)} async-done(((bf16[256,2048]{1,0:T(8,128)(2,1)}), bf16[128,2048]{1,0:T(8,128)(2,1)}) %reduce-scatter.2.cloned.1.call-update) | async-done | bytes 524304 | tf_op jit(solution)/shard_map/reduce_scatter | solution.py:172
  (32 shorter events, 0.2 us)
Async XLA Ops:
  6.5 37.7 %copy-start = (bf16[512,2048]{1,0:T(8,128)(2,1)S(1)}, bf16[512,2048]{1,0:T(8,128)(2,1)}, u32[]{:S(2)}) copy-start(bf16[512,2048]{1,0:T(8,128)(2,1)} %param.26) | copy-start | bytes 6291460
  6.5 17.0 %copy-start.15 = (f32[256]{0:T(256)S(1)}, f32[256]{0:T(256)}, u32[]{:S(2)}) copy-start(f32[256]{0:T(256)} %param.23) | copy-start | bytes 3076
  6.5 17.1 %copy-start.13 = (bf16[2048,32]{0,1:T(8,128)(2,1)S(1)}, bf16[2048,32]{0,1:T(8,128)(2,1)}, u32[]{:S(2)}) copy-start(bf16[2048,32]{0,1:T(8,128)(2,1)} %param.21) | copy-start | bytes 393220
  6.5 13.1 %all-gather.3.cloned.1.call-start = ((), (), s32[]{:S(2)}) async-start(), calls=%async_computation.1 | async-start | bytes 1572864 | tf_op jit(solution)/shard_map/all_gather | solution.py:119
  7.3 85.3 %all-gather.5.cloned.1.call-start = ((), (), s32[]{:S(2)}) async-start(), calls=%async_computation.2 | async-start | bytes 3342336 | tf_op jit(solution)/shard_map/all_gather | solution.py:153
  7.3 18.8 %copy-start.1 = (bf16[256,1024]{1,0:T(8,128)(2,1)S(1)}, bf16[256,1024]{1,0:T(8,128)(2,1)}, u32[]{:S(2)}) copy-start(bf16[256,1024]{1,0:T(8,128)(2,1)} %up_ref.1) | copy-start | bytes 1572868
  19.6 4.1 %copy-start.4 = (bf16[256,2048]{1,0:T(8,128)(2,1)S(1)}, bf16[256,2048]{1,0:T(8,128)(2,1)}, u32[]{:S(2)}) copy-start(bf16[256,2048]{1,0:T(8,128)(2,1)} %all-gather.3.cloned.1.call-done) | copy-start | bytes 3145732
  23.7 2.8 %copy-start.14 = (bf16[3,512]{1,0:T(4,128)(2,1)S(1)}, bf16[3,512]{1,0:T(4,128)(2,1)}, u32[]{:S(2)}) copy-start(bf16[3,512]{1,0:T(4,128)(2,1)} %param.18) | copy-start | bytes 9220
  26.1 121.6 %reduce-scatter.2.cloned.1.call-start = ((), (), s32[]{:S(2)}) async-start(), calls=%async_computation.3 | async-start | bytes 1572864 | tf_op jit(solution)/shard_map/reduce_scatter | solution.py:172
  26.4 4.4 %copy-start.11 = (bf16[512,768]{1,0:T(8,128)(2,1)S(1)}, bf16[512,768]{1,0:T(8,128)(2,1)}, u32[]{:S(2)}) copy-start(bf16[512,768]{1,0:T(8,128)(2,1)} %param.24) | copy-start | bytes 2359300
  28.5 6.6 %copy-start.12 = (f32[256,16]{1,0:T(8,128)S(1)}, f32[256,16]{1,0:T(8,128)}, u32[]{:S(2)}) copy-start(f32[256,16]{1,0:T(8,128)} %get-tuple-element.10) | copy-start | bytes 49156
  35.2 2.9 %copy-start.5 = (bf16[256,2048]{1,0:T(8,128)(2,1)S(1)}, bf16[256,2048]{1,0:T(8,128)(2,1)}, u32[]{:S(2)}) copy-start(bf16[256,2048]{1,0:T(8,128)(2,1)} %all-gather.3.cloned.1.call-done) | copy-start | bytes 3145732
  35.2 3.0 %copy-start.10 = (bf16[2048,512]{1,0:T(8,128)(2,1)S(1)}, bf16[2048,512]{1,0:T(8,128)(2,1)}, u32[]{:S(2)}) copy-start(bf16[2048,512]{1,0:T(8,128)(2,1)} %param.17) | copy-start | bytes 6291460
  38.2 3.8 %copy-start.8 = (f32[256,768]{0,1:T(8,128)S(1)}, f32[256,768]{0,1:T(8,128)}, u32[]{:S(2)}) copy-start(f32[256,768]{0,1:T(8,128)} %copy.24) | copy-start | bytes 2359300
  38.9 5.2 %collective-permute-start = (bf16[2,512]{1,0:T(2,128)(2,1)S(1)}, bf16[2,512]{1,0:T(2,128)(2,1)S(1)}, u32[]{:S(2)}, u32[]{:S(2)}) collective-permute-start(bf16[2,512]{1,0:T(2,128)(2,1)S(1)} %slice.64), channel_id=1, source_target_pairs={{0,2},{2,4},{4,6},{6,8},{8,10},{10,12},{12,14},{14,16},{16,18},{18... | collective-permute-start | bytes 6152 | tf_op jit(solution)/shard_map/ppermute | solution.py:23
  42.2 1.0 copy-start.2
  92.6 1.2 slice-start
  92.6 2.2 %copy-start.7 = (bf16[4096,288]{1,0:T(8,128)(2,1)S(1)}, bf16[4096,288]{1,0:T(8,128)(2,1)}, u32[]{:S(2)}) copy-start(bf16[4096,288]{1,0:T(8,128)(2,1)} %all-gather.5.cloned.1.call-done) | copy-start | bytes 7077892
  94.8 1.2 copy-start.3
  96.0 37.7 %copy-start.6 = (f32[256,2048]{1,0:T(8,128)S(1)}, f32[256,2048]{1,0:T(8,128)}, u32[]{:S(2)}) copy-start(f32[256,2048]{1,0:T(8,128)} %fusion.3) | copy-start | bytes 6291460
  96.0 37.7 %copy-start.9 = (bf16[512,2048]{1,0:T(8,128)(2,1)S(1)}, bf16[512,2048]{1,0:T(8,128)(2,1)}, u32[]{:S(2)}) copy-start(bf16[512,2048]{1,0:T(8,128)(2,1)} %param.27) | copy-start | bytes 6291460
Sparse Core Ops, SparseCore 0:
  8.9 10.6 all-gather.2
  26.2 66.2 all-gather.4
  135.5 12.1 reduce-scatter.1

commit v2 on v1

--- a/solution.py
+++ b/solution.py
@@ -11,6 +11,7 @@
 LANES = 128
 ONES = 16
 
+MESH = pl.DeviceIdType.MESH
 neg_fill = -1e30
 rotary_base = 10000.0
 norm_epsilon = 1e-06
@@ -78,23 +79,209 @@
             best_ref[h] = new
 
 
-def attention_kernel(lat_ref, rot_ref, qx_ref, up_ref, wvt_ref, out_ref, best_ref, acc_ref):
+def mix_kernel(
+    lat_in, rot_in, qx_ref, up_ref, wvt_ref, conv_ref, cproj_ref, aproj_ref, out_ref,
+    lat, rot, best_ref, acc_ref, att, part_buf, in_buf,
+    own_sem, lat_send, lat_recv, rot_send, rot_recv, share_send, share_recv, tail_send, tail_recv,
+):
     me = lax.axis_index("sp")
+    t = lax.axis_index("tp")
+    total = lax.axis_size("sp")
+    ways = lax.axis_size("tp")
+    planes = total // 4
+    z = me // 4
+    b0 = me % 2
+    b1 = (me // 2) % 2
+    a0 = 1 - t % 2
     rows = qx_ref.shape[2]
+    short = rows // ways
+
+    def block_of(plane, ka, kb):
+        f0 = a0 * ka + (1 - a0) * kb
+        f1 = a0 * kb + (1 - a0) * ka
+        return plane * 4 + (b1 + f1 * (1 - 2 * b1)) * 2 + b0 + f0 * (1 - 2 * b0)
+
+    up = lax.rem(me + 4, total)
+    down = lax.rem(me + total - 4, total)
+    a_peer = block_of(z, 1, 0)
+    b_peer = block_of(z, 0, 1)
+    mates = [lax.rem(t + o, ways) for o in range(1, ways)]
+
+    barrier = pltpu.get_barrier_semaphore()
+    for target in [(up, t), (down, t), (a_peer, t), (b_peer, t)] + [(me, mate) for mate in mates]:
+        pl.semaphore_signal(barrier, inc=1, device_id=target, device_id_type=MESH)
+
+    own = [
+        pltpu.make_async_copy(lat_in, lat.at[me], own_sem.at[0]),
+        pltpu.make_async_copy(rot_in, rot.at[me], own_sem.at[1]),
+    ]
+    for copy in own:
+        copy.start()
+    for copy in own:
+        copy.wait()
+    pl.semaphore_wait(barrier, 4 + len(mates))
+
+    def hop(j, k, target):
+        return [
+            pltpu.make_async_remote_copy(
+                buf.at[j, t] if split else buf.at[j],
+                buf.at[j, t] if split else buf.at[j],
+                send.at[j, k],
+                recv.at[j],
+                device_id=(target, t),
+                device_id_type=MESH,
+            )
+            for buf, send, recv, split in ((lat, lat_send, lat_recv, True), (rot, rot_send, rot_recv, False))
+        ]
+
+    def start(j, k, target):
+        for copy in hop(j, k, target):
+            copy.start()
+
+    def arrive(j):
+        for copy in hop(j, 0, up):
+            copy.wait_recv()
+
+    def shares(j):
+        return [
+            pltpu.make_async_remote_copy(
+                lat.at[j, t],
+                lat.at[j, t],
+                share_send.at[j, o],
+                share_recv.at[j, o],
+                device_id=(me, mate),
+                device_id_type=MESH,
+            )
+            for o, mate in enumerate(mates)
+        ]
+
+    def share_landed(j):
+        for o in range(len(mates)):
+            source = lax.rem(t + ways - 1 - o, ways)
+            pltpu.make_async_remote_copy(
+                lat.at[j, source],
+                lat.at[j, source],
+                share_send.at[j, o],
+                share_recv.at[j, o],
+                device_id=(me, mates[o]),
+                device_id_type=MESH,
+            ).wait_recv()
+
+    def share(j):
+        @pl.when(j < me)
+        def _():
+            for copy in shares(j):
+                copy.start()
+
+    def spread(j):
+        @pl.when(z + 1 < planes)
+        def _():
+            start(j, 0, up)
+
+        start(j, 1, a_peer)
+        start(j, 2, b_peer)
+
+    def stage_a(d):
+        j = block_of(z - d, 0, 0)
+        arrive(j)
+        spread(j)
+        share(j)
+
+    def stage_b(d):
+        j = block_of(z - d, 1, 0)
+        arrive(j)
+        start(j, 2, b_peer)
+        share(j)
+
+    def stage_c(d):
+        for ka in (0, 1):
+            j = block_of(z - d, ka, 1)
+            arrive(j)
+            share(j)
 
     def block(j, masked):
-        at = pl.ds(pl.multiple_of(j * rows, rows), rows)
-        attend(lat_ref[at, :], rot_ref[at, :], qx_ref, up_ref, wvt_ref, best_ref, acc_ref, masked)
-
+        latent = jnp.concatenate([lat[j, s] for s in range(ways)], 1)
+        turned = rot[j].astype(jnp.float32)
+        turned = jnp.concatenate([turned, jnp.zeros((LANES - ROPE, rows), jnp.float32)], 0)
+        turned = turned.T.astype(jnp.bfloat16)
+        attend(latent, turned, qx_ref, up_ref, wvt_ref, best_ref, acc_ref, masked)
+
+    spread(me)
     block(me, True)
-
-    @pl.loop(0, me)
-    def _(j):
-        block(j, False)
+    stage_b(0)
+    stage_c(0)
+
+    @pl.loop(0, 4 * (z + 1))
+    def _(n):
+        d = n // 4
+        k = n % 4
+        for order, stage in enumerate((stage_a, stage_b, stage_c)):
+
+            @pl.when(jnp.logical_and(k == order, d < z))
+            def _():
+                stage(d + 1)
+
+        j = block_of(z - d, k % 2, k // 2)
+
+        @pl.when(j < me)
+        def _():
+            share_landed(j)
+            block(j, False)
 
     for h in range(qx_ref.shape[0]):
         acc = acc_ref[h]
-        out_ref[h * VDIM : (h + 1) * VDIM, :] = (acc[:VDIM] / acc[VDIM : VDIM + 1]).astype(jnp.bfloat16)
+        acc_ref[h, :VDIM] = acc[:VDIM] / acc[VDIM : VDIM + 1]
+    flat = jnp.concatenate([acc_ref[h, :VDIM] for h in range(qx_ref.shape[0])], 0)
+    att[...] = flat.T.astype(jnp.bfloat16)
+
+    def part(owner):
+        at = pl.ds(pl.multiple_of(owner * short, short), short)
+        return (dot(conv_ref[at, :], cproj_ref[...]) + dot(att[at, :], aproj_ref[...])).astype(jnp.bfloat16)
+
+    tails = []
+    for o, mate in enumerate(mates):
+        part_buf[o] = part(mate)
+        tails.append(
+            pltpu.make_async_remote_copy(
+                part_buf.at[o],
+                in_buf.at[o],
+                tail_send.at[o],
+                tail_recv.at[o],
+                device_id=(me, mate),
+                device_id_type=MESH,
+            )
+        )
+        tails[-1].start()
+    result = part(t).astype(jnp.float32)
+    for o, copy in enumerate(tails):
+        copy.wait_recv()
+        result = result + in_buf[o].astype(jnp.float32)
+    out_ref[...] = result.astype(jnp.bfloat16)
+    for copy in tails:
+        copy.wait_send()
+
+    @pl.loop(0, z + 1)
+    def _(d):
+        def sent(j, k):
+            for copy in hop(j, k, up):
+                copy.wait_send()
+
+        mine = block_of(z - d, 0, 0)
+
+        @pl.when(z + 1 < planes)
+        def _():
+            sent(mine, 0)
+
+        sent(mine, 1)
+        sent(mine, 2)
+        sent(block_of(z - d, 1, 0), 2)
+        for k in range(4):
+            j = block_of(z - d, k % 2, k // 2)
+
+            @pl.when(j < me)
+            def _():
+                for copy in shares(j):
+                    copy.wait_send()
 
 
 def local(
@@ -149,27 +336,42 @@
         ],
         2,
     ).transpose(1, 2, 0)
-    shared = jnp.concatenate([latent_norm, rotary_key], 1)
-    shared = lax.all_gather(shared, "sp", axis=0, tiled=True)
     kvr = latent_norm.shape[1]
-    keys = shared[:, :kvr]
-    rots = jnp.pad(shared[:, kvr:], ((0, 0), (0, LANES - ROPE)))
+    ways = lax.axis_size("tp")
+    blocks = lax.axis_size("sp")
+    model = conv_project.shape[1]
+    pieces = latent_norm.reshape(rows, ways, kvr // ways).transpose(1, 0, 2)
     wvt = latent_up.reshape(kvr, heads, NOPE + VDIM)[..., NOPE:].reshape(kvr, heads * VDIM).T
     vmem = pl.BlockSpec(memory_space=pltpu.VMEM)
-    attended = pl.pallas_call(
-        attention_kernel,
-        out_shape=jax.ShapeDtypeStruct((heads * VDIM, rows), jnp.bfloat16),
-        in_specs=[vmem] * 5,
+    dma = pltpu.SemaphoreType.DMA
+    mates = ways - 1
+    return pl.pallas_call(
+        mix_kernel,
+        out_shape=jax.ShapeDtypeStruct((rows // ways, model), jnp.bfloat16),
+        in_specs=[vmem] * 8,
         out_specs=vmem,
         scratch_shapes=[
+            pltpu.VMEM((blocks, ways, rows, kvr // ways), jnp.bfloat16),
+            pltpu.VMEM((blocks, ROPE, rows), jnp.bfloat16),
             pltpu.VMEM((heads, 1, rows), jnp.float32),
             pltpu.VMEM((heads, VDIM + ONES, rows), jnp.float32),
+            pltpu.VMEM((rows, heads * VDIM), jnp.bfloat16),
+            pltpu.VMEM((mates, rows // ways, model), jnp.bfloat16),
+            pltpu.VMEM((mates, rows // ways, model), jnp.bfloat16),
+            dma((2,)),
+            dma((blocks, 3)),
+            dma((blocks,)),
+            dma((blocks, 3)),
+            dma((blocks,)),
+            dma((blocks, mates)),
+            dma((blocks, mates)),
+            dma((mates,)),
+            dma((mates,)),
         ],
-        compiler_params=pltpu.CompilerParams(vmem_limit_bytes=48 * 1024 * 1024),
-    )(keys, rots, qx, latent_up, wvt)
-    partial = jnp.dot(conv_result, conv_project, preferred_element_type=jnp.float32)
-    partial = partial + dot(attended, attend_project, ((0,), (0,)))
-    return lax.psum_scatter(partial.astype(jnp.bfloat16), "tp", scatter_dimension=0, tiled=True)
+        compiler_params=pltpu.CompilerParams(
+            vmem_limit_bytes=56 * 1024 * 1024, collective_id=0, has_side_effects=True
+        ),
+    )(pieces, rotary_key.T, qx, latent_up, wvt, conv_result, conv_project, attend_project)
 
 
 def solution(mesh):

time: 156 us -> 119 us (0.76); the launches traced: 154 us -> 119 us
  waiting for transfers between devices: 70 us -> 9.3 us
  Pallas kernels: 37.6 us -> 63 us
  matrix products: 16.3 us -> 9.9 us
  local copies, waits for them, and re-layouts: 7.3 us -> 11.8 us
  other arithmetic: 2.49 us -> 4.27 us
    all_gather x1 -> x0, waiting for transfers between devices: 43.7 us -> none  [local(): shared = lax.all_gather(shared, 'sp', axis=0, tiled=True)]
    pallas_call x1, Pallas kernels: 37.6 us -> 63 us  [local(): pl.pallas_call(mix_kernel, out_shape=jax.ShapeDtypeStruct((rows // ways,...]
    reduce_scatter x1 -> x0, waiting for transfers between devices: 12.3 us -> none  [local(): lax.psum_scatter(partial.astype(jnp.bfloat16), 'tp', scatter_dimension=0,...]
    dot_general x2 -> x0, matrix products: 6.39 us -> none  [the longest x1 4.67 us: local(): jnp.dot(conv_result, conv_project, preferred_element_type=jnp.float32)]
    all_gather x1, waiting for transfers between devices: 12.2 us -> 8.59 us  [local(): piece = lax.all_gather(tokens, 'tp', axis=1, tiled=True)]
    unnamed x34 -> x27, local copies, waits for them, and re-layouts: 3.06 us -> 4.32 us
    dot_general x5 -> x6, matrix products: 7.87 us -> 8.57 us  [local(): jnp.dot(piece, weight, preferred_element_type=jnp.float32)]
  transfers between devices with their start and end apart: 4 -> 2, of which waited for: 4 -> 1; matrix products, arithmetic and copies ran while one was open for 10% -> 9% of each run, Pallas kernels for 0% -> 0%
where the time goes in v2:
time: 119 us
  Pallas kernels  63 us (53%)
  between operations  13.6 us (11%)
  local copies, waits for them, and re-layouts  11.8 us (10%)
  matrix products  9.9 us (8%)
  waiting for transfers between devices  9.3 us (8%)
  other arithmetic  4.27 us (4%)
  blocking collectives  4.06 us (3%)
  starting transfers between devices  3.1 us (3%)
    pallas_call x1, Pallas kernels, local(): pl.pallas_call(mix_kernel, out_shape=jax.ShapeDtypeStruct((rows // ways,...  63 us
    all_gather x1, waiting for transfers between devices, local(): piece = lax.all_gather(tokens, 'tp', axis=1, tiled=True)  8.59 us
    dot_general x6, matrix products, local(): jnp.dot(piece, weight, preferred_element_type=jnp.float32)  8.57 us
    unnamed x27, local copies, waits for them, and re-layouts  4.32 us
    ppermute x1, starting transfers between devices, shifted(): return lax.ppermute(shard, axis, pairs)  3.1 us
  transfers between devices with their start and end apart: 2, of which 1 were waited for; matrix products, arithmetic and copies ran while one was open for 9% of the time, Pallas kernels for 0%

profile of v2, /device:TPU:29, one launch (start us, length us, event | category | flops | bytes accessed | tf_op | source)
XLA Modules:
  0.0 119.0 jit_solution(101072120606270145)
XLA Ops:
  6.5 0.0 copy-start
  6.5 0.0 all-gather.2.cloned.1.call-start
  6.5 0.7 all-gather.2.cloned.1.call-update
  7.3 1.3 %copy.21 = bf16[256,1024]{0,1:T(8,128)(2,1)S(1)} copy(bf16[256,1024]{1,0:T(8,128)(2,1)} %up_ref.1) | data formatting | bytes 1048576 | tf_op jit(solution)/shard_map/reshape | solution.py:344
  8.6 0.7 slice.61
  9.3 0.6 negate_power_fusion
  9.9 0.5 add_convert_fusion.2
  10.4 0.0 copy-done.7
  10.4 0.6 fusion.16
  11.0 8.6 %all-gather.2.cloned.1.call-done = bf16[256,2048]{1,0:T(8,128)(2,1)} async-done(((bf16[256,1024]{1,0:T(8,128)(2,1)}), bf16[256,2048]{1,0:T(8,128)(2,1)}) %all-gather.2.cloned.1.call-update) | async-done | bytes 1048592 | tf_op jit(solution)/shard_map/all_gather | solution.py:306
  19.6 0.0 copy-done.5
  19.6 1.7 %convolution_convert_fusion.1 = bf16[256,128]{1,0:T(8,128)(2,1)S(1)} fusion(bf16[256,2048]{1,0:T(8,128)(2,1)} %all-gather.2.cloned.1.call-done, bf16[2048,128]{1,0:T(8,128)(2,1)S(1)} %copy-done.5), kind=kOutput, calls=%fused_computation.6 | convolution fusion | flops 134250496 | bytes 1638400 | tf_op jit(solution)/shard_map/dot_general | solution.py:308
  21.3 1.9 %all_gather.10 = bf16[256,256]{1,0:T(8,128)(2,1)S(1)} all-gather(bf16[256,128]{1,0:T(8,128)(2,1)S(1)} %convolution_convert_fusion.1), channel_id=1, replica_groups=mesh['sp'=16,'tp'=2] {'tp'}, dimensions={1}, use_global_device_ids=true | all-gather | bytes 196608 | tf_op jit(solution)/shard_map/all_gather | solution.py:311
  23.3 0.1 fusion.7
  23.4 2.0 %convolution_convert_fusion = bf16[256,256]{1,0:T(8,128)(2,1)S(1)} fusion(bf16[256,2048]{1,0:T(8,128)(2,1)} %all-gather.2.cloned.1.call-done, bf16[2048,256]{1,0:T(8,128)(2,1)} %param.19), kind=kOutput, calls=%fused_computation.5 | convolution fusion | flops 268500992 | bytes 2228224 | tf_op jit(solution)/shard_map/dot_general | solution.py:308
  25.4 0.0 copy-start.1
  25.4 2.1 %all_gather.11 = bf16[256,512]{1,0:T(8,128)(2,1)S(1)} all-gather(bf16[256,256]{1,0:T(8,128)(2,1)S(1)} %convolution_convert_fusion), channel_id=1, replica_groups=mesh['sp'=16,'tp'=2] {'tp'}, dimensions={1}, use_global_device_ids=true | all-gather | bytes 393216 | tf_op jit(solution)/shard_map/all_gather | solution.py:310
  27.5 0.1 fusion.2
  27.6 0.0 copy-done.8
  27.7 0.0 copy-done.4
  27.7 1.3 %convolution_multiply_fusion = f32[256,768]{1,0:T(8,128)} fusion(bf16[512,768]{1,0:T(8,128)(2,1)S(1)} %copy-done.4, bf16[256,512]{1,0:T(8,128)(2,1)S(1)} %all_gather.11, f32[512]{0:T(512)S(1)} %copy-done.8, f32[256]{0:T(256)S(1)} %add_rsqrt_fusion), kind=kOutput, calls=%fused_computation | convolution fusion | flops 202047488 | bytes 1838080 | tf_op jit(solution)/shard_map/dot_general | solution.py:326
  29.0 2.3 %copy.19 = f32[256,768]{0,1:T(8,128)} copy(f32[256,768]{1,0:T(8,128)} %convolution_multiply_fusion) | data formatting | bytes 1572864 | tf_op jit(solution)/shard_map/mul | solution.py:326
  31.3 0.7 fusion.18
  32.0 0.9 copy-done.3
  32.9 0.7 fusion.1
  33.6 0.0 copy-start.9
  33.7 3.1 %collective-permute-start = (bf16[2,512]{1,0:T(2,128)(2,1)S(1)}, bf16[2,512]{1,0:T(2,128)(2,1)S(1)}, u32[]{:S(2)}, u32[]{:S(2)}) collective-permute-start(bf16[2,512]{1,0:T(2,128)(2,1)S(1)} %slice.62), channel_id=1, source_target_pairs={{0,2},{2,4},{4,6},{6,8},{8,10},{10,12},{12,14},{14,16},{16,18},{18... | collective-permute-start | bytes 6152 | tf_op jit(solution)/shard_map/ppermute | solution.py:24
  36.8 0.0 copy-done.2
  36.8 0.8 fusion.10
  37.5 0.7 broadcast_dynamic-update-slice_fusion.1
  38.3 0.0 copy-done.6
  38.3 0.4 fusion.17
  38.7 0.0 copy-done.10
  38.7 0.0 copy-done.11
  38.7 0.1 multiply_cosine_fusion
  38.9 0.7 fusion.14
  39.5 0.7 fusion.15
  40.2 0.8 broadcast_dynamic-update-slice_fusion
  41.0 0.0 copy-done.9
  41.0 0.7 fusion.9
  41.8 0.6 maximum_bitcast_fusion.rot_in
  42.4 1.0 copy.17
  43.4 0.8 copy.18
  44.1 0.0 collective-permute-done
  44.1 0.1 maximum_convert_fusion
  44.2 3.1 %fusion.conv_ref = bf16[256,512]{1,0:T(8,128)(2,1)} fusion(bf16[256,2048]{1,0:T(8,128)(2,1)S(1)} %copy-done.1, bf16[2048,512]{1,0:T(8,128)(2,1)} %param.15, f32[258,512]{1,0:T(8,128)S(1)} %maximum_convert_fusion, f32[512]{0:T(512)} %bitcast.35, f32[512]{0:T(512)} %bitcast.34, f32[512]{0:T(512)S(1)} %bitcast.33), kind=kOutput, calls=%fused_computation.3 | convolution fusion | flops 537788416 | bytes 4986880 | tf_op jit(solution)/shard_map/dot_general | solution.py:308
  47.3 63.0 %shard_map.136 = bf16[128,2048]{1,0:T(8,128)(2,1)} custom-call(bf16[2,256,128]{2,1,0:T(8,128)(2,1)} %bitcast.31, bf16[32,256]{1,0:T(8,128)(2,1)} %maximum_bitcast_fusion.rot_in, bf16[8,256,256]{2,1,0:T(8,128)(2,1)} %bitcast.4.qx_ref, bf16[256,1024]{1,0:T(8,128)(2,1)} %up_ref.1, bf16[512,256]{1,0:T(8,128)(2,1)} %bitcast.30, bf16[256,512]{1,0:T(8,128)(2,1)} %fusion.conv_ref, ...), custom_call_target="tpu_custom_call" | custom-call | tf_op jit(solution)/shard_map/pallas_call | solution.py:348
  110.3 1.9 %copy.27 = bf16[128,2048]{1,0:T(8,128)(2,1)} copy(bf16[128,2048]{1,0:T(8,128)(2,1)} %shard_map.136) | data formatting | bytes 1048576
  (14 shorter events, 0.0 us)
Async XLA Ops:
  6.5 24.8 %copy-start = (bf16[2048,512]{1,0:T(8,128)(2,1)S(1)}, bf16[2048,512]{1,0:T(8,128)(2,1)}, u32[]{:S(2)}) copy-start(bf16[2048,512]{1,0:T(8,128)(2,1)} %param.16) | copy-start | bytes 6291460
  6.5 3.9 %copy-start.7 = (bf16[3,512]{1,0:T(4,128)(2,1)S(1)}, bf16[3,512]{1,0:T(4,128)(2,1)}, u32[]{:S(2)}) copy-start(bf16[3,512]{1,0:T(4,128)(2,1)} %param.18) | copy-start | bytes 9220
  6.5 13.1 %copy-start.5 = (bf16[2048,128]{1,0:T(8,128)(2,1)S(1)}, bf16[2048,128]{1,0:T(8,128)(2,1)}, u32[]{:S(2)}) copy-start(bf16[2048,128]{1,0:T(8,128)(2,1)} %param.20) | copy-start | bytes 1572868
  6.5 13.1 %all-gather.2.cloned.1.call-start = ((), (), s32[]{:S(2)}) async-start(), calls=%async_computation | async-start | bytes 1572864 | tf_op jit(solution)/shard_map/all_gather | solution.py:306
  11.0 16.6 %copy-start.8 = (f32[512]{0:T(512)S(1)}, f32[512]{0:T(512)}, u32[]{:S(2)}) copy-start(f32[512]{0:T(512)} %param.22) | copy-start | bytes 6148
  19.6 8.1 %copy-start.4 = (bf16[512,768]{1,0:T(8,128)(2,1)S(1)}, bf16[512,768]{1,0:T(8,128)(2,1)}, u32[]{:S(2)}) copy-start(bf16[512,768]{1,0:T(8,128)(2,1)} %param.24) | copy-start | bytes 2359300
  25.4 6.0 %copy-start.1 = (bf16[256,2048]{1,0:T(8,128)(2,1)S(1)}, bf16[256,2048]{1,0:T(8,128)(2,1)}, u32[]{:S(2)}) copy-start(bf16[256,2048]{1,0:T(8,128)(2,1)} %all-gather.2.cloned.1.call-done) | copy-start | bytes 3145732
  31.3 1.6 %copy-start.3 = (bf16[2048,512]{1,0:T(8,128)(2,1)S(1)}, bf16[2048,512]{1,0:T(8,128)(2,1)}, u32[]{:S(2)}) copy-start(bf16[2048,512]{1,0:T(8,128)(2,1)} %param.17) | copy-start | bytes 6291460
  32.9 3.9 %copy-start.2 = (f32[256,768]{0,1:T(8,128)S(1)}, f32[256,768]{0,1:T(8,128)}, u32[]{:S(2)}) copy-start(f32[256,768]{0,1:T(8,128)} %copy.19) | copy-start | bytes 2359300
  32.9 5.4 %copy-start.6 = (bf16[2048,32]{0,1:T(8,128)(2,1)S(1)}, bf16[2048,32]{0,1:T(8,128)(2,1)}, u32[]{:S(2)}) copy-start(bf16[2048,32]{0,1:T(8,128)(2,1)} %param.21) | copy-start | bytes 393220
  32.9 5.8 %copy-start.10 = (f32[256]{0:T(256)S(1)}, f32[256]{0:T(256)}, u32[]{:S(2)}) copy-start(f32[256]{0:T(256)} %add_convert_fusion.2) | copy-start | bytes 3076
  32.9 5.8 %copy-start.11 = (f32[16]{0:T(128)S(1)}, f32[16]{0:T(128)}, u32[]{:S(2)}) copy-start(f32[16]{0:T(128)} %negate_power_fusion) | copy-start | bytes 196
  33.6 7.4 %copy-start.9 = (f32[256]{0:T(256)S(1)}, f32[256]{0:T(256)}, u32[]{:S(2)}) copy-start(f32[256]{0:T(256)} %param.23) | copy-start | bytes 3076
  33.7 10.5 %collective-permute-start = (bf16[2,512]{1,0:T(2,128)(2,1)S(1)}, bf16[2,512]{1,0:T(2,128)(2,1)S(1)}, u32[]{:S(2)}, u32[]{:S(2)}) collective-permute-start(bf16[2,512]{1,0:T(2,128)(2,1)S(1)} %slice.62), channel_id=1, source_target_pairs={{0,2},{2,4},{4,6},{6,8},{8,10},{10,12},{12,14},{14,16},{16,18},{18... | collective-permute-start | bytes 6152 | tf_op jit(solution)/shard_map/ppermute | solution.py:24
Sparse Core Ops, SparseCore 0:
  8.9 10.6 all-gather.1

commit v3 on v2

--- a/solution.py
+++ b/solution.py
@@ -10,42 +10,13 @@
 VDIM = 64
 LANES = 128
 ONES = 16
+EDGE = 16
 
 MESH = pl.DeviceIdType.MESH
 neg_fill = -1e30
 rotary_base = 10000.0
 norm_epsilon = 1e-06
 log2e = 1.4426950408889634
-
-
-def shifted(shard, axis, by):
-    length = lax.axis_size(axis)
-    pairs = [(i, i + by) for i in range(length) if 0 <= i + by < length]
-    return lax.ppermute(shard, axis, pairs)
-
-
-def angles(positions):
-    half = ROPE // 2
-    inverse = rotary_base ** (-(jnp.arange(half, dtype=jnp.float32) * 2.0 / (2 * half)))
-    return positions[:, None] * inverse[None, :]
-
-
-def rotate(values, positions):
-    half = values.shape[-1] // 2
-    angle = angles(positions)
-    if values.ndim == 3:
-        angle = angle[:, None, :]
-    cosine = jnp.cos(angle)
-    sine = jnp.sin(angle)
-    first = values[..., :half]
-    second = values[..., half:]
-    return jnp.concatenate([first * cosine - second * sine, first * sine + second * cosine], -1)
-
-
-def rms_scale(latent, gain):
-    values = latent.astype(jnp.float32)
-    factor = lax.rsqrt(jnp.mean(values * values, -1, keepdims=True) + norm_epsilon)
-    return (values * factor * gain).astype(jnp.bfloat16)
 
 
 def dot(a, b, dims=((1,), (0,))):
@@ -80,9 +51,13 @@
 
 
 def mix_kernel(
-    lat_in, rot_in, qx_ref, up_ref, wvt_ref, conv_ref, cproj_ref, aproj_ref, out_ref,
+    tok, inv_ref, taps_ref, qgain_ref, lgain_ref,
+    ldown_in, qdown_in, rdown_in, inner_in, signal_in, outer_in, qup_in, up_in, cproj_in, aproj_in,
+    out_ref,
+    ldown, qdown, rdown, inner_w, signal_w, outer_w, qup, up_ref, cproj_ref, aproj_ref,
+    xbuf, raw_lat, raw_query, edge, rim, padded, conv_ref, wvt_ref, qx_ref,
     lat, rot, best_ref, acc_ref, att, part_buf, in_buf,
-    own_sem, lat_send, lat_recv, rot_send, rot_recv, share_send, share_recv, tail_send, tail_recv,
+    load_sem, front_send, front_recv, lat_send, lat_recv, rot_send, rot_recv, share_send, share_recv, tail_send, tail_recv,
 ):
     me = lax.axis_index("sp")
     t = lax.axis_index("tp")
@@ -103,23 +78,93 @@
 
     up = lax.rem(me + 4, total)
     down = lax.rem(me + total - 4, total)
+    after = lax.rem(me + 1, total)
+    before = lax.rem(me + total - 1, total)
     a_peer = block_of(z, 1, 0)
     b_peer = block_of(z, 0, 1)
     mates = [lax.rem(t + o, ways) for o in range(1, ways)]
 
     barrier = pltpu.get_barrier_semaphore()
-    for target in [(up, t), (down, t), (a_peer, t), (b_peer, t)] + [(me, mate) for mate in mates]:
+    for target in [(up, t), (down, t), (a_peer, t), (b_peer, t), (after, t), (before, t)] + [(me, mate) for mate in mates]:
         pl.semaphore_signal(barrier, inc=1, device_id=target, device_id_type=MESH)
 
-    own = [
-        pltpu.make_async_copy(lat_in, lat.at[me], own_sem.at[0]),
-        pltpu.make_async_copy(rot_in, rot.at[me], own_sem.at[1]),
-    ]
-    for copy in own:
+    pairs = (
+        (ldown_in, ldown), (qdown_in, qdown), (rdown_in, rdown), (inner_in, inner_w), (signal_in, signal_w),
+        (outer_in, outer_w), (qup_in, qup), (up_in, up_ref), (cproj_in, cproj_ref), (aproj_in, aproj_ref),
+    )
+    loads = [pltpu.make_async_copy(a, b, load_sem.at[i]) for i, (a, b) in enumerate(pairs)]
+    for copy in loads:
         copy.start()
-    for copy in own:
+    pl.semaphore_wait(barrier, 6 + len(mates))
+
+    def to_mates(source, slots, kind):
+        return [
+            pltpu.make_async_remote_copy(
+                source, slots.at[o], front_send.at[kind, o], front_recv.at[kind, o],
+                device_id=(me, mate), device_id_type=MESH,
+            )
+            for o, mate in enumerate(mates)
+        ]
+
+    token_sends = to_mates(tok, xbuf, 0)
+    for copy in token_sends:
+        copy.start()
+    depth = tok.shape[1]
+
+    def rows_from(weight, o):
+        at = pl.multiple_of(lax.rem(t + ways - o, ways) * depth, depth)
+        return weight[pl.ds(at, depth), :]
+
+    def rest(value, weight):
+        for o in range(1, ways):
+            value = value + dot(xbuf[o - 1], rows_from(weight, o))
+        return value
+
+    for copy in loads[:3]:
         copy.wait()
-    pl.semaphore_wait(barrier, 4 + len(mates))
+    first = [dot(tok[...], rows_from(weight, 0)) for weight in (ldown, qdown, rdown)]
+    for copy in token_sends:
+        copy.wait_recv()
+    lat_part, query_part, turn_part = [rest(v, w) for v, w in zip(first, (ldown, qdown, rdown))]
+    raw_lat[ways - 1] = lat_part.astype(jnp.bfloat16)
+    raw_query[ways - 1] = query_part.astype(jnp.bfloat16)
+    latent_sends = to_mates(raw_lat.at[ways - 1], raw_lat, 1) + to_mates(raw_query.at[ways - 1], raw_query, 2)
+    for copy in latent_sends:
+        copy.start()
+
+    position = (me * rows + lax.broadcasted_iota(jnp.int32, (1, rows), 1)).astype(jnp.float32)
+    angle = inv_ref[...] * position
+    cosine = jnp.cos(angle)
+    sine = jnp.sin(angle)
+    half = ROPE // 2
+
+    def rotated(values):
+        a = values[:half]
+        b = values[half:]
+        return jnp.concatenate([a * cosine - b * sine, a * sine + b * cosine], 0).astype(jnp.bfloat16)
+
+    turn = jnp.concatenate([turn_part, jnp.zeros((rows, LANES - ROPE), jnp.float32)], 1).T
+    rot[me] = rotated(turn[:ROPE])
+
+    loads[3].wait()
+    loads[4].wait()
+    inner = rest(dot(tok[...], rows_from(inner_w, 0)), inner_w)
+    signal = rest(dot(tok[...], rows_from(signal_w, 0)), signal_w)
+    gated = (inner * signal).astype(jnp.bfloat16)
+    padded[EDGE:] = gated.astype(jnp.float32)
+    edge[...] = gated[rows - EDGE :]
+
+    def whole(raw, gain_ref):
+        values = jnp.concatenate([raw[lax.rem(t + ways - 1 - s, ways)] for s in range(ways)], 1).astype(jnp.float32)
+        factor = lax.rsqrt(jnp.mean(values * values, -1, keepdims=True) + norm_epsilon)
+        return (values * factor * gain_ref[...]).astype(jnp.bfloat16)
+
+    for copy in latent_sends:
+        copy.wait_recv()
+    latent_norm = whole(raw_lat, lgain_ref)
+    wide = latent_norm.shape[1] // ways
+    for s in range(ways):
+        lat[me, s] = latent_norm[:, s * wide : (s + 1) * wide]
 
     def hop(j, k, target):
         return [
@@ -207,8 +252,49 @@
         attend(latent, turned, qx_ref, up_ref, wvt_ref, best_ref, acc_ref, masked)
 
     spread(me)
+    rim_copy = pltpu.make_async_remote_copy(
+        edge, rim, front_send.at[3, 0], front_recv.at[3, 0], device_id=(after, t), device_id_type=MESH
+    )
+
+    @pl.when(me + 1 < total)
+    def _():
+        rim_copy.start()
+
+    loads[6].wait()
+    loads[7].wait()
+    scale = (NOPE + ROPE) ** (-0.5) * log2e
+    query = (dot(whole(raw_query, qgain_ref), qup[...]) * scale).T
+    heads = qx_ref.shape[0]
+    size = NOPE + ROPE
+    turned_up = up_ref[...].astype(jnp.float32).T.astype(jnp.bfloat16)
+    for h in range(heads):
+        base = h * size
+        qx_ref[h, :NOPE] = query[base : base + NOPE].astype(jnp.bfloat16)
+        qx_ref[h, NOPE : NOPE + VDIM] = jnp.zeros((VDIM, rows), jnp.bfloat16)
+        qx_ref[h, NOPE + VDIM : NOPE + VDIM + ROPE] = rotated(query[base + NOPE : base + size])
+        qx_ref[h, NOPE + VDIM + ROPE :] = jnp.zeros((LANES - ROPE, rows), jnp.bfloat16)
+        low = h * (NOPE + VDIM) + NOPE
+        wvt_ref[h * VDIM : (h + 1) * VDIM] = turned_up[low : low + VDIM]
+
     block(me, True)
     stage_b(0)
+    loads[5].wait()
+    outer = rest(dot(tok[...], rows_from(outer_w, 0)), outer_w)
+
+    @pl.when(me > 0)
+    def _():
+        rim_copy.wait_recv()
+        padded[:EDGE] = rim[...].astype(jnp.float32)
+
+    @pl.when(me == 0)
+    def _():
+        padded[:EDGE] = jnp.zeros((EDGE, padded.shape[1]), jnp.float32)
+
+    reach = taps_ref.shape[0] - 1
+    filtered = padded[EDGE:] * taps_ref[reach : reach + 1, :]
+    for k in range(reach):
+        filtered = filtered + padded[EDGE - reach + k : EDGE - reach + k + rows] * taps_ref[k : k + 1, :]
+    conv_ref[...] = (outer * filtered).astype(jnp.bfloat16)
     stage_c(0)
 
     @pl.loop(0, 4 * (z + 1))
@@ -233,6 +319,9 @@
         acc_ref[h, :VDIM] = acc[:VDIM] / acc[VDIM : VDIM + 1]
     flat = jnp.concatenate([acc_ref[h, :VDIM] for h in range(qx_ref.shape[0])], 0)
     att[...] = flat.T.astype(jnp.bfloat16)
+
+    loads[8].wait()
+    loads[9].wait()
 
     def part(owner):
         at = pl.ds(pl.multiple_of(owner * short, short), short)
@@ -257,8 +346,12 @@
         copy.wait_recv()
         result = result + in_buf[o].astype(jnp.float32)
     out_ref[...] = result.astype(jnp.bfloat16)
-    for copy in tails:
+    for copy in tails + token_sends + latent_sends:
         copy.wait_send()
+
+    @pl.when(me + 1 < total)
+    def _():
+        rim_copy.wait_send()
 
     @pl.loop(0, z + 1)
     def _(d):
@@ -302,63 +395,53 @@
 ):
     rows = tokens.shape[0]
     heads = query_up.shape[1] // (NOPE + ROPE)
-    weights = (outer_gate, inner_gate, conv_input, query_down, latent_down, rotary_down)
-    piece = lax.all_gather(tokens, "tp", axis=1, tiled=True)
-    outer, inner, signal, query_part, latent_part, rotary_raw = tuple(
-        (jnp.dot(piece, weight, preferred_element_type=jnp.float32) for weight in weights)
-    )
-    query_lat = lax.all_gather(query_part.astype(jnp.bfloat16), "tp", axis=1, tiled=True)
-    latent_lat = lax.all_gather(latent_part.astype(jnp.bfloat16), "tp", axis=1, tiled=True)
-    gated = (inner * signal).astype(jnp.bfloat16)
-    reach = conv_taps.shape[0] - 1
-    rim = shifted(gated[rows - reach :], "sp", 1)
-    padded = jnp.concatenate([rim, gated], 0).astype(jnp.float32)
-    taps = conv_taps.astype(jnp.float32)
-    filtered = padded[0:rows] * taps[0]
-    for index in range(1, reach + 1):
-        filtered = filtered + padded[index : index + rows] * taps[index]
-    conv_result = (outer * filtered).astype(jnp.bfloat16)
-    positions = (lax.axis_index("sp") * rows + jnp.arange(rows, dtype=jnp.int32)).astype(jnp.float32)
-    query_norm = rms_scale(query_lat, query_gain)
-    latent_norm = rms_scale(latent_lat, latent_gain)
-    rotary_key = rotate(rotary_raw, positions).astype(jnp.bfloat16)
-    scale = (NOPE + ROPE) ** (-0.5) * log2e
-    query = jnp.dot(query_norm, query_up, preferred_element_type=jnp.float32) * scale
-    query = query.reshape(rows, heads, NOPE + ROPE)
-    plain = query[..., :NOPE].astype(jnp.bfloat16)
-    turned = rotate(query[..., NOPE:], positions).astype(jnp.bfloat16)
-    qx = jnp.concatenate(
-        [
-            plain,
-            jnp.zeros((rows, heads, VDIM), jnp.bfloat16),
-            turned,
-            jnp.zeros((rows, heads, LANES - ROPE), jnp.bfloat16),
-        ],
-        2,
-    ).transpose(1, 2, 0)
-    kvr = latent_norm.shape[1]
     ways = lax.axis_size("tp")
     blocks = lax.axis_size("sp")
     model = conv_project.shape[1]
-    pieces = latent_norm.reshape(rows, ways, kvr // ways).transpose(1, 0, 2)
-    wvt = latent_up.reshape(kvr, heads, NOPE + VDIM)[..., NOPE:].reshape(kvr, heads * VDIM).T
+    kvr = latent_up.shape[0]
+    channels = conv_project.shape[0]
+    half = ROPE // 2
+    inverse = rotary_base ** (-(jnp.arange(half, dtype=jnp.float32) * 2.0 / (2 * half)))
     vmem = pl.BlockSpec(memory_space=pltpu.VMEM)
     dma = pltpu.SemaphoreType.DMA
     mates = ways - 1
+    big = (
+        latent_down, query_down, rotary_down, inner_gate, conv_input,
+        outer_gate, query_up, latent_up, conv_project, attend_project,
+    )
+
+    def half_type(*shape):
+        return pltpu.VMEM(shape, jnp.bfloat16)
+
+    def full_type(*shape):
+        return pltpu.VMEM(shape, jnp.float32)
+
     return pl.pallas_call(
         mix_kernel,
         out_shape=jax.ShapeDtypeStruct((rows // ways, model), jnp.bfloat16),
-        in_specs=[vmem] * 8,
+        in_specs=[vmem] * 5 + [pl.BlockSpec(memory_space=pl.ANY)] * len(big),
         out_specs=vmem,
-        scratch_shapes=[
-            pltpu.VMEM((blocks, ways, rows, kvr // ways), jnp.bfloat16),
-            pltpu.VMEM((blocks, ROPE, rows), jnp.bfloat16),
-            pltpu.VMEM((heads, 1, rows), jnp.float32),
-            pltpu.VMEM((heads, VDIM + ONES, rows), jnp.float32),
-            pltpu.VMEM((rows, heads * VDIM), jnp.bfloat16),
-            pltpu.VMEM((mates, rows // ways, model), jnp.bfloat16),
-            pltpu.VMEM((mates, rows // ways, model), jnp.bfloat16),
-            dma((2,)),
+        scratch_shapes=[half_type(*array.shape) for array in big]
+        + [
+            half_type(mates, *tokens.shape),
+            half_type(ways, rows, latent_down.shape[1]),
+            half_type(ways, rows, query_down.shape[1]),
+            half_type(EDGE, channels),
+            half_type(EDGE, channels),
+            full_type(EDGE + rows, channels),
+            half_type(rows, channels),
+            half_type(heads * VDIM, kvr),
+            half_type(heads, NOPE + VDIM + LANES, rows),
+            half_type(blocks, ways, rows, kvr // ways),
+            half_type(blocks, ROPE, rows),
+            full_type(heads, 1, rows),
+            full_type(heads, VDIM + ONES, rows),
+            half_type(rows, heads * VDIM),
+            half_type(mates, rows // ways, model),
+            half_type(mates, rows // ways, model),
+            dma((len(big),)),
+            dma((4, mates)),
+            dma((4, mates)),
             dma((blocks, 3)),
             dma((blocks,)),
             dma((blocks, 3)),
@@ -369,9 +452,16 @@
             dma((mates,)),
         ],
         compiler_params=pltpu.CompilerParams(
-            vmem_limit_bytes=56 * 1024 * 1024, collective_id=0, has_side_effects=True
+            vmem_limit_bytes=60 * 1024 * 1024, collective_id=0, has_side_effects=True
         ),
-    )(pieces, rotary_key.T, qx, latent_up, wvt, conv_result, conv_project, attend_project)
+    )(
+        tokens,
+        inverse[:, None],
+        conv_taps.astype(jnp.float32),
+        query_gain[None, :],
+        latent_gain[None, :],
+        *big,
+    )
 
 
 def solution(mesh):

time: 119 us -> 72.8 us (0.61)
  between operations: 13.6 us -> 0.01 us
  matrix products: 9.9 us -> 0 us
  waiting for transfers between devices: 9.3 us -> 0 us
  local copies, waits for them, and re-layouts: 11.8 us -> 3.79 us
  blocking collectives: 4.06 us -> 0 us
  Pallas kernels: 63 us -> 66.9 us
  starting transfers between devices: 3.1 us -> 0 us
  other arithmetic: 4.27 us -> 1.89 us
    dot_general x7 -> x0, matrix products: 9.9 us -> none  [the longest x6 8.57 us: local(): jnp.dot(piece, weight, preferred_element_type=jnp.float32)]
    all_gather x1 -> x0, waiting for transfers between devices: 8.59 us -> none  [local(): piece = lax.all_gather(tokens, 'tp', axis=1, tiled=True)]
    all_gather x2 -> x0, blocking collectives: 4.06 us -> none  [the longest x1 2.13 us: local(): lax.all_gather(query_part.astype(jnp.bfloat16), 'tp', axis=1, tiled=True)]
    pallas_call x1, Pallas kernels: 63 us -> 66.9 us  [local(): pl.pallas_call(mix_kernel, out_shape=jax.ShapeDtypeStruct((rows // ways,...]
    ppermute x1 -> x0, starting transfers between devices: 3.1 us -> none  [shifted(): return lax.ppermute(shard, axis, pairs)]
    mul x1 -> x0, local copies, waits for them, and re-layouts: 2.32 us -> none  [local(): jnp.dot(query_norm, query_up, preferred_element_type=jnp.float32) * scale]
    reshape x2 -> x0, local copies, waits for them, and re-layouts: 2.06 us -> none  [the longest x1 1.3 us: local(): latent_up.reshape(kvr, heads, NOPE + VDIM)[..., NOPE:]]
    unnamed x2 -> x0, other arithmetic: 1.33 us -> none
  transfers between devices with their start and end apart: 2 -> 0, of which waited for: 1 -> 0; matrix products, arithmetic and copies ran while one was open for 9% -> 0% of each run, Pallas kernels for 0% -> 0%
where the time goes in v3:
time: 72.8 us; the launch traced here: 72.6 us
  Pallas kernels  66.9 us (92%)
  local copies, waits for them, and re-layouts  3.79 us (5%)
  other arithmetic  1.89 us (3%)
    pallas_call x1, Pallas kernels, local(): pl.pallas_call(mix_kernel, out_shape=jax.ShapeDtypeStruct((rows // ways,...  66.9 us
    unnamed x2, local copies, waits for them, and re-layouts  3.79 us

profile of v3, /device:TPU:29, one launch (start us, length us, event | category | flops | bytes accessed | tf_op | source)
XLA Modules:
  0.0 72.6 jit_solution(5898787937229868873)
XLA Ops:
  0.0 1.3 %convert_element_type.3.taps_ref = f32[3,512]{1,0:T(4,128)} convert(bf16[3,512]{1,0:T(4,128)(2,1)} %param.18) | non-fusion elementwise | flops 1536 | bytes 9216 | tf_op jit(solution)/shard_map/convert_element_type | solution.py:460
  1.3 0.6 negate_power_fusion.inv_ref
  1.9 1.9 %copy.15.rdown_in = bf16[2048,32]{1,0:T(8,128)(2,1)} copy(bf16[2048,32]{0,1:T(8,128)(2,1)} %param.21) | data formatting | bytes 262144 | tf_op args[7]
  3.8 66.9 %shard_map.136 = bf16[128,2048]{1,0:T(8,128)(2,1)} custom-call(bf16[256,1024]{1,0:T(8,128)(2,1)} %tok.1, f32[16,1]{1,0:T(8,128)} %negate_power_fusion.inv_ref, f32[3,512]{1,0:T(4,128)} %convert_element_type.3.taps_ref, f32[1,512]{1,0:T(1,128)} %bitcast.2, f32[1,256]{1,0:T(1,128)} %bitcast.3, bf16[2048,128]{1,0:T(8,128)(2,1)} %ldown_in.1, ...), custom_call_target="tpu_custom_call" | custom-call | tf_op jit(solution)/shard_map/pallas_call | solution.py:419
  70.7 1.9 %copy.17 = bf16[128,2048]{1,0:T(8,128)(2,1)} copy(bf16[128,2048]{1,0:T(8,128)(2,1)} %shard_map.136) | data formatting | bytes 1048576

commit v4 on v3

--- a/solution.py
+++ b/solution.py
@@ -1,4 +1,5 @@
 import jax
+import numpy as np
 import jax.numpy as jnp
 from jax import lax
 from jax.experimental import pallas as pl
@@ -39,13 +40,13 @@
         values = jnp.concatenate([turned[h * VDIM : (h + 1) * VDIM], ones], 0)
         top = jnp.max(s, 0, keepdims=True)
         if masked:
-            weight = jnp.exp2(s - top).astype(jnp.bfloat16)
+            weight = jnp.exp2((s - top).astype(jnp.bfloat16))
             acc_ref[h] = dot(values, weight)
             best_ref[h] = top
         else:
             old = best_ref[h]
             new = jnp.maximum(old, top)
-            weight = jnp.exp2(s - new).astype(jnp.bfloat16)
+            weight = jnp.exp2((s - new).astype(jnp.bfloat16))
             acc_ref[h] = acc_ref[h] * jnp.exp2(old - new) + dot(values, weight)
             best_ref[h] = new
 
@@ -113,16 +114,21 @@
 
     def rows_from(weight, o):
         at = pl.multiple_of(lax.rem(t + ways - o, ways) * depth, depth)
+        if weight is rdown:
+            return weight[:, pl.ds(at, depth)]
         return weight[pl.ds(at, depth), :]
+
+    def project(x, weight, o):
+        return dot(x, rows_from(weight, o), ((1,), (1 if weight is rdown else 0,)))
 
     def rest(value, weight):
         for o in range(1, ways):
-            value = value + dot(xbuf[o - 1], rows_from(weight, o))
+            value = value + project(xbuf[o - 1], weight, o)
         return value
 
     for copy in loads[:3]:
         copy.wait()
-    first = [dot(tok[...], rows_from(weight, 0)) for weight in (ldown, qdown, rdown)]
+    first = [project(tok[...], weight, 0) for weight in (ldown, qdown, rdown)]
     for copy in token_sends:
         copy.wait_recv()
     lat_part, query_part, turn_part = [rest(v, w) for v, w in zip(first, (ldown, qdown, rdown))]
@@ -291,9 +297,10 @@
         padded[:EDGE] = jnp.zeros((EDGE, padded.shape[1]), jnp.float32)
 
     reach = taps_ref.shape[0] - 1
-    filtered = padded[EDGE:] * taps_ref[reach : reach + 1, :]
+    taps = taps_ref[...].astype(jnp.float32)
+    filtered = padded[EDGE:] * taps[reach : reach + 1, :]
     for k in range(reach):
-        filtered = filtered + padded[EDGE - reach + k : EDGE - reach + k + rows] * taps_ref[k : k + 1, :]
+        filtered = filtered + padded[EDGE - reach + k : EDGE - reach + k + rows] * taps[k : k + 1, :]
     conv_ref[...] = (outer * filtered).astype(jnp.bfloat16)
     stage_c(0)
 
@@ -401,12 +408,12 @@
     kvr = latent_up.shape[0]
     channels = conv_project.shape[0]
     half = ROPE // 2
-    inverse = rotary_base ** (-(jnp.arange(half, dtype=jnp.float32) * 2.0 / (2 * half)))
+    inverse = jnp.asarray(np.float32(rotary_base) ** (-(np.arange(half, dtype=np.float32) * 2.0 / (2 * half))), jnp.float32)
     vmem = pl.BlockSpec(memory_space=pltpu.VMEM)
     dma = pltpu.SemaphoreType.DMA
     mates = ways - 1
     big = (
-        latent_down, query_down, rotary_down, inner_gate, conv_input,
+        latent_down, query_down, rotary_down.T, inner_gate, conv_input,
         outer_gate, query_up, latent_up, conv_project, attend_project,
     )
 
@@ -457,7 +464,7 @@
     )(
         tokens,
         inverse[:, None],
-        conv_taps.astype(jnp.float32),
+        conv_taps,
         query_gain[None, :],
         latent_gain[None, :],
         *big,

time: 72.8 us -> 69.7 us (0.957)
  local copies, waits for them, and re-layouts: 3.79 us -> 1.88 us
  other arithmetic: 1.89 us -> 0 us
    unnamed x2 -> x1, local copies, waits for them, and re-layouts: 3.79 us -> 1.88 us
    convert_element_type x1 -> x0, other arithmetic: 1.28 us -> none  [local(): conv_taps.astype(jnp.float32)]
    pallas_call x1, Pallas kernels: 66.9 us -> 67.6 us  [local(): pl.pallas_call(mix_kernel, out_shape=jax.ShapeDtypeStruct((rows // ways,...]
where the time goes in v4:
time: 69.7 us; the launch traced here: 69.5 us
  Pallas kernels  67.6 us (97%)
  local copies, waits for them, and re-layouts  1.88 us (3%)
    pallas_call x1, Pallas kernels, local(): pl.pallas_call(mix_kernel, out_shape=jax.ShapeDtypeStruct((rows // ways,...  67.6 us
    unnamed x1, local copies, waits for them, and re-layouts  1.88 us

profile of v4, /device:TPU:29, one launch (start us, length us, event | category | flops | bytes accessed | tf_op | source)
XLA Modules:
  0.0 69.5 jit_solution(17236011099774139375)
XLA Ops:
  0.0 67.6 %shard_map.145 = bf16[128,2048]{1,0:T(8,128)(2,1)} custom-call(bf16[256,1024]{1,0:T(8,128)(2,1)} %tok.1, f32[16,1]{1,0:T(8,128)} %constant.3.inv_ref, bf16[3,512]{1,0:T(4,128)(2,1)} %taps_ref.1, f32[1,512]{1,0:T(1,128)} %bitcast.4, f32[1,256]{1,0:T(1,128)} %bitcast.5, bf16[2048,128]{1,0:T(8,128)(2,1)} %ldown_in.1, bf16[2048,256]{1,0:T(8,128)(2,1)} %qdown_in.1, ...), custom_call_target="tpu_custom_call" | custom-call | tf_op jit(solution)/shard_map/pallas_call | solution.py:426
  67.6 1.9 %copy.17 = bf16[128,2048]{1,0:T(8,128)(2,1)} copy(bf16[128,2048]{1,0:T(8,128)(2,1)} %shard_map.145) | data formatting | bytes 1048576
